TPU v7x, 512 devices: a whole 4x4x16 slice. The times are simulated.
512 devices in a mesh: gr: 2 (over z_hi), fs: 32 (over z_lo, y), tp: 8 (over x, core).
Axes of the slice: x: 4, y: 4, z: 16 (z_hi: 2, z_lo: 8; z = z_hi * 8 + z_lo), core: 2. Of those that a mesh axis runs over, the one named last changes fastest.
Arguments:
- tokens: bfloat16 [8192, 2048], P(('gr', 'fs')), may hold values from -60 to 60
- route_ids: int32 [8192, 2], P(('gr', 'fs')), may hold values from 0 to 7, all different within a row; in each aligned block of 128 rows (0 to 127, 128 to 255, ...) at most 32 rows name the same one
- route_logits: float32 [8192, 2], P(('gr', 'fs')), may hold values from -8 to 8
- norm_gain: float32 [2048], P(('gr', 'fs')), may hold values from 0.1 to 1.9
- gate_master: float32 [8, 2048, 7168], P(None, ('gr', 'fs'), 'tp'), may hold values from -0.125 to 0.125
- up_master: float32 [8, 2048, 7168], P(None, ('gr', 'fs'), 'tp'), may hold values from -0.125 to 0.125
- down_master: float32 [8, 7168, 2048], P(None, 'fs', ('gr', 'tp')), may hold values from -0.0625 to 0.0625
Outputs:
- gate_weight: bfloat16 [8, 2048, 7168], P('tp', None, 'fs')
- up_weight: bfloat16 [8, 2048, 7168], P('tp', None, 'fs')
- down_weight: bfloat16 [8, 7168, 2048], P('tp', 'fs')
- mixed: bfloat16 [8192, 2048], P(('gr', 'fs'))
Inputs may be any that keep to these rules, and one draw needn't show every extreme that they name: `route_ids`: in the rows of one device, that is in each aligned block of 128 rows, each of the 8 experts is named by exactly 32 rows; a row names two different experts.
All inputs are finite; a program needn't handle non-finite values.
Results may differ from a plain program's by a relative error of at most 0.025.
Values may be sent and summed in bfloat16 or wider, within the bound.
No kernel may reach another device: no remote copies, remote signals or barrier semaphores. Data moves between devices by JAX's collectives and lax.ppermute only.
A program may use at most 64 MiB of HBM per device.

v0:
```python
import jax
import jax.numpy as jnp
from jax import lax
from jax.experimental import pallas as pl
from jax.experimental.pallas import tpu as pltpu
from jax.sharding import Mesh
from jax.sharding import PartitionSpec as P


CAP = 32
FS = ("fs_0", "fs_1")
GR_FS = ("gr", "fs_0", "fs_1")
ALL = ("gr", "fs_0", "fs_1", "tp")
EPS = 1e-06
LANES = 128


def lane_window(blocks, start):
    first, offset = divmod(start, LANES)
    if offset == 0:
        return blocks[first]
    head = pltpu.roll(blocks[first], LANES - offset, 1)
    if first + 1 == len(blocks):
        return head
    rest = pltpu.roll(blocks[first + 1], LANES - offset, 1)
    lane = lax.broadcasted_iota(jnp.int32, head.shape, 1)
    return jnp.where(lane < LANES - offset, head, rest)


def pack_kernel(gate_ref, up_ref, gain_ref, out_ref):
    gain = gain_ref[...]
    both = jnp.concatenate([gate_ref[0] * gain, up_ref[0] * gain], axis=0)
    blocks = [both[:, LANES * b : LANES * (b + 1)] for b in range(both.shape[1] // LANES)]
    lane = lax.broadcasted_iota(jnp.int32, (48, LANES), 1)
    for j in range(4):
        main = lane_window(blocks, 224 * j)
        tail = lane_window(blocks, 224 * j + LANES)
        last = tail[48:]
        spread = jnp.concatenate([pltpu.roll(last, 96 - 32 * q, 1) for q in range(3)], axis=0)
        out_ref[0, 112 * j : 112 * j + 64, :] = main.astype(jnp.bfloat16)
        out_ref[0, 112 * j + 64 : 112 * j + 112, :] = jnp.where(lane < 96, tail[:48], spread).astype(jnp.bfloat16)


def pack(gate_master, up_master, gain):
    experts, rows, cols = gate_master.shape
    return pl.pallas_call(
        pack_kernel,
        grid=(experts,),
        in_specs=[
            pl.BlockSpec((1, rows, cols), lambda i: (i, 0, 0)),
            pl.BlockSpec((1, rows, cols), lambda i: (i, 0, 0)),
            pl.BlockSpec((rows, 1), lambda i: (0, 0)),
        ],
        out_specs=pl.BlockSpec((1, 448, LANES), lambda i: (i, 0, 0)),
        out_shape=jax.ShapeDtypeStruct((experts, 448, LANES), jnp.bfloat16),
        cost_estimate=pl.CostEstimate(flops=4000000, bytes_accessed=2800000, transcendentals=0),
        compiler_params=pltpu.CompilerParams(vmem_limit_bytes=58 * 2**20),
        name="pack",
    )(gate_master, up_master, gain)


def hidden_kernel(tiles_ref, tokens_ref, gate_ref, up_ref, even_ref, odd_ref):
    @pl.when(pl.program_id(0) == 0)
    def _():
        lane = lax.broadcasted_iota(jnp.int32, (16, LANES), 1)

        def unpack(s, carry):
            rows = pl.ds(pl.multiple_of(32 * s, 32), 32)
            gate_ref[0, rows, :LANES] = tiles_ref[s, 0:32, :]
            up_ref[0, rows, :LANES] = tiles_ref[s, 32:64, :]
            gate_ref[0, rows, LANES:] = tiles_ref[s, 64:96, :96]
            up_ref[0, pl.ds(pl.multiple_of(32 * s, 16), 16), LANES:] = tiles_ref[s, 96:112, :96]
            parts = [
                pltpu.roll(
                    tiles_ref[s, 64 + 16 * q : 80 + 16 * q, :].astype(jnp.float32), 32 * q + 32, 1
                )
                for q in range(3)
            ]
            last = jnp.where(lane < 32, parts[0], jnp.where(lane < 64, parts[1], parts[2]))
            rest = pl.ds(pl.multiple_of(32 * s + 16, 16), 16)
            up_ref[0, rest, LANES:] = last[:, :96].astype(jnp.bfloat16)
            return carry

        lax.fori_loop(0, tiles_ref.shape[0], unpack, 0, unroll=4)

    tokens = tokens_ref[...]
    gate = jnp.dot(tokens, gate_ref[0], preferred_element_type=jnp.float32)
    up = jnp.dot(tokens, up_ref[0], preferred_element_type=jnp.float32)
    hidden = (gate / (1.0 + jnp.exp(-gate)) * up).astype(jnp.bfloat16)
    half = hidden.shape[0] // 2
    even_ref[0] = hidden[:half]
    for k in range(odd_ref.shape[0]):
        odd_ref[k, 0, :, :224] = hidden[half:]
        odd_ref[k, 0, :, 224:] = jnp.zeros((half, 32), jnp.bfloat16)


def hidden_units(tiles, tokens, pieces):
    count = tiles.shape[0]
    rows = tokens.shape[0] // pieces
    weight = jax.ShapeDtypeStruct((1, 32 * count, 224), jnp.bfloat16)
    even = jax.ShapeDtypeStruct((pieces, rows // 2, 224), jnp.bfloat16)
    odd = jax.ShapeDtypeStruct((pieces, pieces, rows // 2, 256), jnp.bfloat16)
    return pl.pallas_call(
        hidden_kernel,
        grid=(pieces,),
        in_specs=[
            pl.BlockSpec(tiles.shape, lambda i: (0, 0, 0)),
            pl.BlockSpec((rows, tokens.shape[1]), lambda i: (i, 0)),
        ],
        out_specs=[pl.BlockSpec(weight.shape, lambda i: (0, 0, 0))] * 2
        + [
            pl.BlockSpec((1, rows // 2, 224), lambda i: (i, 0, 0)),
            pl.BlockSpec((pieces, 1, rows // 2, 256), lambda i: (0, i, 0, 0)),
        ],
        out_shape=[weight, weight, even, odd],
        cost_estimate=pl.CostEstimate(
            flops=1900000000, bytes_accessed=8500000, transcendentals=230000
        ),
        compiler_params=pltpu.CompilerParams(
            dimension_semantics=("arbitrary",), vmem_limit_bytes=58 * 2**20
        ),
        name="hidden_units",
    )(tiles, tokens)


def out_kernel(*refs):
    out_ref = refs[-1]
    count = (len(refs) - 1) // 2
    for i in range(out_ref.shape[0]):
        total = jnp.dot(refs[0][i], refs[count][...], preferred_element_type=jnp.float32)
        for k in range(1, count):
            total = total + jnp.dot(
                refs[k][i], refs[count + k][...], preferred_element_type=jnp.float32
            )
        out_ref[i] = total.astype(out_ref.dtype)


def all_out_kernel(row_ref, hidden_ref, *refs):
    out_ref = refs[-1]
    count = hidden_ref.shape[0]
    for i in range(out_ref.shape[0]):
        total = jnp.dot(
            hidden_ref[row_ref[0], i, :, :224], refs[0][...], preferred_element_type=jnp.float32
        )
        for k in range(1, count):
            source = lax.rem(row_ref[0] + (count - k), count)
            total = total + jnp.dot(
                hidden_ref[source, i, :, :224], refs[k][...], preferred_element_type=jnp.float32
            )
        out_ref[i] = total.astype(out_ref.dtype)


def partial_out(hidden, down, kind, row=None):
    shape = (*hidden[0].shape[-3:-1], down[0].shape[1])
    whole = pl.BlockSpec(memory_space=pltpu.VMEM)
    first = [] if row is None else [row]
    return pl.pallas_call(
        out_kernel if row is None else all_out_kernel,
        in_specs=[pl.BlockSpec(memory_space=pltpu.SMEM)] * len(first)
        + [whole] * (len(hidden) + len(down)),
        out_specs=whole,
        out_shape=jax.ShapeDtypeStruct(shape, kind),
        cost_estimate=pl.CostEstimate(
            flops=470000000, bytes_accessed=3000000, transcendentals=0
        ),
        compiler_params=pltpu.CompilerParams(vmem_limit_bytes=12 * 2**20),
        name="partial_out",
    )(*first, *hidden, *down)


def permutation(sizes, move):
    groups, fs_0, fs_1, tp = sizes
    pairs = []
    for g in range(groups):
        for a in range(fs_0):
            for b in range(fs_1):
                for t in range(tp):
                    z, y = move(g * fs_0 + a, b, t)
                    z, y = z % (groups * fs_0), y % fs_1
                    pairs.append((((g * fs_0 + a) * fs_1 + b) * tp + t, (z * fs_1 + y) * tp + t))
    return pairs


def local(sizes, tokens, route_ids, route_logits, norm_gain, gate_master, up_master, down_master):
    f32, bf16 = jnp.float32, jnp.bfloat16
    fs_1, tp_size = sizes[2], sizes[3]

    def along_z(x, hops):
        pairs = permutation(sizes, lambda z, y, t: (z + (hops if t % 2 == 0 else -hops), y))
        return lax.ppermute(x, ALL, pairs)

    def along_y(x, hops):
        return lax.ppermute(x, ALL, permutation(sizes, lambda z, y, t: (z, y + hops)))

    as_float = tokens.astype(f32)
    normed = (
        as_float * lax.rsqrt(jnp.mean(as_float * as_float, axis=-1, keepdims=True) + EPS)
    ).astype(bf16)
    differ = route_logits[:, 0] - route_logits[:, 1]
    route_weight = jnp.stack([jax.nn.sigmoid(differ), jax.nn.sigmoid(-differ)], axis=1)
    expert_ids = jnp.arange(tp_size, dtype=jnp.int32)
    route_hits = route_ids[None, :, :] == expert_ids[:, None, None]
    chosen = jnp.any(route_hits, axis=2)
    slot_rank = jnp.cumsum(chosen.astype(jnp.int32), axis=1) - 1
    slot_ids = jnp.arange(CAP, dtype=jnp.int32)
    picker = chosen[:, None, :] & (slot_rank[:, None, :] == slot_ids[None, :, None])
    weight_rows = jnp.sum(jnp.where(route_hits, route_weight[None, :, :], 0.0), axis=2)
    mine = lax.axis_index("tp")
    my_picker = lax.dynamic_index_in_dim(picker, mine, 0, keepdims=False)
    slot_weight = jnp.sum(jnp.where(picker, weight_rows[:, None, :], 0.0), axis=2)
    packed = jnp.dot(my_picker.astype(bf16), normed, preferred_element_type=f32).astype(bf16)

    down_tiles = down_master.astype(bf16)
    down_tiles = lax.all_to_all(down_tiles, "tp", 0, 0, tiled=True)
    down_own = jnp.moveaxis(down_tiles, 0, 1).reshape(down_tiles.shape[1], -1)
    across = permutation(sizes, lambda z, y, t: (z + sizes[1], y))
    down_other = lax.ppermute(down_own, ALL, across)

    tiles = pack(gate_master, up_master, norm_gain[:, None])
    tiles = lax.all_to_all(tiles, "tp", 0, 0, tiled=True).reshape(-1, 112, LANES)
    tiles = jnp.concatenate([tiles, tiles], axis=0)
    tiles = lax.all_to_all(tiles, GR_FS, 0, 0, tiled=True)

    held = packed
    for hops in (4, 2, 1):
        moved = along_z(held, hops)
        held = jnp.concatenate([held, moved], axis=0)
    row = lax.axis_index("fs_1")
    gathered = jnp.zeros((fs_1, *held.shape), bf16)
    for k in range(fs_1):
        moved = held
        if k:
            moved = along_y(held, k)
        gathered = lax.dynamic_update_index_in_dim(gathered, moved, (row + fs_1 - k) % fs_1, 0)
    gathered = gathered.reshape(-1, gathered.shape[2])
    low = lax.axis_index("gr") == 0
    down_weight = jnp.concatenate(
        [jnp.where(low, down_own, down_other), jnp.where(low, down_other, down_own)], axis=1
    )
    columns = down_weight.shape[1] // fs_1
    down_cols = []
    for k in range(fs_1):
        picked = lax.dynamic_slice_in_dim(down_weight, (row + k) % fs_1 * columns, columns, axis=1)
        if k:
            picked = along_y(picked, k)
        down_cols.append(picked)
    tiles, gathered = lax.optimization_barrier((tiles, gathered))
    gate_weight, up_weight, even, odd = hidden_units(tiles, gathered, fs_1)

    odd = lax.all_to_all(odd, "fs_1", 0, 0, tiled=True)
    pieces = [even]
    for k in range(1, fs_1):
        pieces.append(along_y(even, k))
    odd = partial_out([odd], down_cols, bf16, row.astype(jnp.int32)[None])
    total = partial_out(pieces, down_cols, f32)
    for hops in (1, 2, 4):
        moved = along_z(odd.astype(bf16), -hops)
        total = total + moved.astype(f32)
        half = total.shape[1] // 2
        total, odd = total[:, :half], total[:, half:]
        if hops == 4:
            total = jnp.concatenate([total, odd], axis=1)

    block = total.astype(bf16)
    block = jnp.broadcast_to(block[:, None], (fs_1, tp_size, *block.shape[1:]))
    blocks = lax.all_to_all(block.reshape(-1, *block.shape[2:]), ("fs_1", "tp"), 0, 0, tiled=True)
    blocks = blocks.reshape(fs_1, -1, columns).astype(f32) * slot_weight.reshape(1, -1, 1)
    blocks = jnp.moveaxis(blocks.astype(bf16), 0, 1).reshape(-1, fs_1 * columns)
    mixed = lax.dot_general(
        picker.reshape(-1, picker.shape[2]).astype(bf16),
        blocks,
        (((0,), (0,)), ((), ())),
        preferred_element_type=f32,
    ).astype(bf16)
    return (gate_weight, up_weight, down_weight[None], mixed)


def solution(mesh):
    sizes = (mesh.shape["gr"], 8, 4, mesh.shape["tp"])
    torus = Mesh(mesh.devices.reshape(sizes), ALL)
    in_specs = (
        P(GR_FS, None),
        P(GR_FS, None),
        P(GR_FS, None),
        P(GR_FS),
        P(None, GR_FS, "tp"),
        P(None, GR_FS, "tp"),
        P(None, FS, ("gr", "tp")),
    )
    out_specs = (P("tp", None, FS), P("tp", None, FS), P("tp", FS, None), P(GR_FS, None))

    def call(*arrays):
        return local(sizes, *arrays)

    return jax.shard_map(call, mesh=torus, in_specs=in_specs, out_specs=out_specs, check_vma=False)
```

profile of v0, /device:TPU:1, one launch (start us, length us, event | category | flops | bytes accessed | tf_op | source)
XLA Modules:
  0.0 335.8 jit_solution(4950997143992938271)
XLA Ops:
  0.6 1.3 copy.30.gain_ref
  2.0 6.3 %pack.1 = bf16[8,448,128]{2,1,0:T(8,128)(2,1)} custom-call(f32[8,32,896]{2,1,0:T(8,128)} %gate_ref.1, f32[8,32,896]{2,1,0:T(8,128)} %up_ref.1, f32[32,1]{1,0:T(8,128)} %copy.30.gain_ref), custom_call_target="tpu_custom_call" | custom-call | flops 4000000 | bytes 2800000 | tf_op jit(solution)/shard_map/pack/pallas_call | solution.py:46
  8.3 10.3 %all-to-all-start = ((bf16[8,448,128]{2,1,0:T(8,128)(2,1)}), bf16[8,448,128]{2,1,0:T(8,128)(2,1)S(1)}, u32[]{:S(2)}, u32[]{:S(2)}) async-start(bf16[8,448,128]{2,1,0:T(8,128)(2,1)} %pack.1), calls=%async_computation | async-start | bytes 1835008 | tf_op jit(solution)/shard_map/all_to_all | solution.py:220
  19.4 12.8 %all-to-all-done = bf16[8,448,128]{2,1,0:T(8,128)(2,1)S(1)} async-done(((bf16[8,448,128]{2,1,0:T(8,128)(2,1)}), bf16[8,448,128]{2,1,0:T(8,128)(2,1)S(1)}, u32[]{:S(2)}, u32[]{:S(2)}) %all-to-all-start) | async-done | bytes 917536 | tf_op jit(solution)/shard_map/all_to_all | solution.py:220
  32.2 4.3 %all-to-all-start.2 = ((bf16[8,224,128]{2,1,0:T(8,128)(2,1)}), bf16[8,224,128]{2,1,0:T(8,128)(2,1)S(1)}, u32[]{:S(2)}, u32[]{:S(2)}) async-start(bf16[8,224,128]{2,1,0:T(8,128)(2,1)} %convert_element_type.51), calls=%async_computation.2 | async-start | bytes 917504 | tf_op jit(solution)/shard_map/all_to_all | solution.py:214
  36.5 1.4 pad_maximum_fusion
  37.9 7.3 %all-to-all-done.2 = bf16[8,224,128]{2,1,0:T(8,128)(2,1)S(1)} async-done(((bf16[8,224,128]{2,1,0:T(8,128)(2,1)}), bf16[8,224,128]{2,1,0:T(8,128)(2,1)S(1)}, u32[]{:S(2)}, u32[]{:S(2)}) %all-to-all-start.2) | async-done | bytes 458784 | tf_op jit(solution)/shard_map/all_to_all | solution.py:214
  45.2 13.9 %all-to-all-start.1 = ((bf16[64,112,128]{2,1,0:T(8,128)(2,1)}), bf16[64,112,128]{2,1,0:T(8,128)(2,1)S(1)}, u32[]{:S(2)}, u32[]{:S(2)}) async-start(bf16[64,112,128]{2,1,0:T(8,128)(2,1)} %pad_maximum_fusion), calls=%async_computation.1 | async-start | bytes 3670016 | tf_op jit(solution)/shard_map/all_to_all | solution.py:222
  60.0 7.0 %collective-permute-start = (bf16[32,2048]{1,0:T(8,128)(2,1)S(1)}, bf16[32,2048]{1,0:T(8,128)(2,1)S(1)}, u32[]{:S(2)}, u32[]{:S(2)}) collective-permute-start(bf16[32,2048]{1,0:T(8,128)(2,1)S(1)} %convolution_convert_fusion.1), channel_id=1, source_target_pairs={{0,128},{1,385},{2,130},{3,387},{4,132},{5,389},{6,134},{7,391},{8... | collective-permute-start | bytes 393224 | tf_op jit(solution)/shard_map/ppermute | solution.py:190
  67.0 81.2 %collective-permute-done = bf16[32,2048]{1,0:T(8,128)(2,1)S(1)} collective-permute-done((bf16[32,2048]{1,0:T(8,128)(2,1)S(1)}, bf16[32,2048]{1,0:T(8,128)(2,1)S(1)}, u32[]{:S(2)}, u32[]{:S(2)}) %collective-permute-start) | collective-permute-done | bytes 131104 | tf_op jit(solution)/shard_map/ppermute | solution.py:190
  148.2 1.9 collective-permute-start.1
  150.2 7.4 %collective-permute-done.1 = bf16[64,2048]{1,0:T(8,128)(2,1)S(1)} collective-permute-done((bf16[64,2048]{1,0:T(8,128)(2,1)S(1)}, bf16[64,2048]{1,0:T(8,128)(2,1)S(1)}, u32[]{:S(2)}, u32[]{:S(2)}) %collective-permute-start.1) | collective-permute-done | bytes 262176 | tf_op jit(solution)/shard_map/ppermute | solution.py:190
  157.6 4.2 %collective-permute-start.2 = (bf16[128,2048]{1,0:T(8,128)(2,1)S(1)}, bf16[128,2048]{1,0:T(8,128)(2,1)S(1)}, u32[]{:S(2)}, u32[]{:S(2)}) collective-permute-start(bf16[128,2048]{1,0:T(8,128)(2,1)S(1)} %pad_maximum_fusion.3), channel_id=1, source_target_pairs={{0,32},{1,481},{2,34},{3,483},{4,36},{5,485},{6,38},{7,487},{8,40}... | collective-permute-start | bytes 1572872 | tf_op jit(solution)/shard_map/ppermute | solution.py:190
  161.8 7.1 %collective-permute-done.2 = bf16[128,2048]{1,0:T(8,128)(2,1)S(1)} collective-permute-done((bf16[128,2048]{1,0:T(8,128)(2,1)S(1)}, bf16[128,2048]{1,0:T(8,128)(2,1)S(1)}, u32[]{:S(2)}, u32[]{:S(2)}) %collective-permute-start.2) | collective-permute-done | bytes 524320 | tf_op jit(solution)/shard_map/ppermute | solution.py:190
  169.9 3.0 collective-permute-start.3
  172.9 5.3 %collective-permute-start.4 = (bf16[256,2048]{1,0:T(8,128)(2,1)}, bf16[256,2048]{1,0:T(8,128)(2,1)}, u32[]{:S(2)}, u32[]{:S(2)}) collective-permute-start(bf16[256,2048]{1,0:T(8,128)(2,1)} %pad_maximum_fusion.2), channel_id=1, source_target_pairs={{0,16},{1,17},{2,18},{3,19},{4,20},{5,21},{6,22},{7,23},{8,24},{9,... | collective-permute-start | bytes 3145736 | tf_op jit(solution)/shard_map/ppermute | solution.py:193
  179.2 8.0 %collective-permute-start.6 = (bf16[224,1024]{1,0:T(8,128)(2,1)}, bf16[224,1024]{1,0:T(8,128)(2,1)}, u32[]{:S(2)}, u32[]{:S(2)}) collective-permute-start(bf16[224,1024]{1,0:T(8,128)(2,1)} %copy_bitcast_fusion), channel_id=1, source_target_pairs={{0,256},{1,257},{2,258},{3,259},{4,260},{5,261},{6,262},{7,263},{8... | collective-permute-start | bytes 1376264 | tf_op jit(solution)/shard_map/ppermute | solution.py:217
  187.2 1.9 collective-permute-start.5
  189.1 2.5 broadcast_in_dim.64
  192.6 1.6 collective-permute-done.3
  194.2 2.3 bitcast_dynamic-update-slice_fusion.2
  196.5 21.5 %collective-permute-done.4 = bf16[256,2048]{1,0:T(8,128)(2,1)} collective-permute-done((bf16[256,2048]{1,0:T(8,128)(2,1)}, bf16[256,2048]{1,0:T(8,128)(2,1)}, u32[]{:S(2)}, u32[]{:S(2)}) %collective-permute-start.4) | collective-permute-done | bytes 1048608 | tf_op jit(solution)/shard_map/ppermute | solution.py:193
  218.0 2.3 bitcast_dynamic-update-slice_fusion.1
  220.4 2.7 collective-permute-done.5
  224.1 1.2 copy-done.2
  225.3 7.7 %hidden_units.1 = (bf16[1,2048,224]{2,1,0:T(8,128)(2,1)}, bf16[1,2048,224]{2,1,0:T(8,128)(2,1)}, bf16[4,128,224]{2,1,0:T(8,128)(2,1)}, bf16[4,4,128,256]{3,2,1,0:T(8,128)(2,1)}) custom-call(bf16[64,112,128]{2,1,0:T(8,128)(2,1)} %copy-done.2, bf16[1024,2048]{1,0:T(8,128)(2,1)} %bitcast.7.tokens_ref), custom_call_target="tpu_custom_call" | custom-call | flops 1900000000 | bytes 8500000 | tf_op jit(solution)/shard_map/hidden_units/pallas_call | solution.py:103
  233.0 4.6 %all-to-all-start.3 = ((bf16[4,4,128,256]{3,2,1,0:T(8,128)(2,1)}), bf16[4,4,128,256]{3,2,1,0:T(8,128)(2,1)S(1)}, u32[]{:S(2)}, u32[]{:S(2)}) async-start(bf16[4,4,128,256]{3,2,1,0:T(8,128)(2,1)} %get-tuple-element.15), calls=%async_computation.3 | async-start | bytes 2097152 | tf_op jit(solution)/shard_map/all_to_all | solution.py:250
  237.6 1.2 broadcast_select_fusion.1
  239.4 3.4 %collective-permute-start.10 = (bf16[224,512]{1,0:T(8,128)(2,1)S(1)}, bf16[224,512]{1,0:T(8,128)(2,1)S(1)}, u32[]{:S(2)}, u32[]{:S(2)}) collective-permute-start(bf16[224,512]{1,0:T(8,128)(2,1)S(1)} %get-tuple-element.34), channel_id=1, source_target_pairs={{0,8},{1,9},{2,10},{3,11},{4,12},{5,13},{6,14},{7,15},{8,16},{9,17... | collective-permute-start | bytes 688136 | tf_op jit(solution)/shard_map/ppermute | solution.py:193
  242.8 4.3 %collective-permute-start.11 = (bf16[224,512]{1,0:T(8,128)(2,1)S(1)}, bf16[224,512]{1,0:T(8,128)(2,1)S(1)}, u32[]{:S(2)}, u32[]{:S(2)}) collective-permute-start(bf16[224,512]{1,0:T(8,128)(2,1)S(1)} %get-tuple-element.35), channel_id=1, source_target_pairs={{0,16},{1,17},{2,18},{3,19},{4,20},{5,21},{6,22},{7,23},{8,24},{9,... | collective-permute-start | bytes 688136 | tf_op jit(solution)/shard_map/ppermute | solution.py:193
  247.1 3.1 collective-permute-start.12
  250.2 5.8 %collective-permute-done.10.refs_5_.refs_1_ = bf16[224,512]{1,0:T(8,128)(2,1)S(1)} collective-permute-done((bf16[224,512]{1,0:T(8,128)(2,1)S(1)}, bf16[224,512]{1,0:T(8,128)(2,1)S(1)}, u32[]{:S(2)}, u32[]{:S(2)}) %collective-permute-start.10) | collective-permute-done | bytes 229408 | tf_op jit(solution)/shard_map/ppermute | solution.py:193
  256.0 5.3 %collective-permute-done.11.refs_6_.refs_2_ = bf16[224,512]{1,0:T(8,128)(2,1)S(1)} collective-permute-done((bf16[224,512]{1,0:T(8,128)(2,1)S(1)}, bf16[224,512]{1,0:T(8,128)(2,1)S(1)}, u32[]{:S(2)}, u32[]{:S(2)}) %collective-permute-start.11) | collective-permute-done | bytes 229408 | tf_op jit(solution)/shard_map/ppermute | solution.py:193
  262.0 4.1 %collective-permute-start.13 = (bf16[4,128,512]{2,1,0:T(8,128)(2,1)S(1)}, bf16[4,128,512]{2,1,0:T(8,128)(2,1)S(1)}, u32[]{:S(2)}, u32[]{:S(2)}) collective-permute-start(bf16[4,128,512]{2,1,0:T(8,128)(2,1)S(1)} %partial_out.3), channel_id=1, source_target_pairs={{0,480},{1,33},{2,482},{3,35},{4,484},{5,37},{6,486},{7,39},{8,488... | collective-permute-start | bytes 1572872 | tf_op jit(solution)/shard_map/ppermute | solution.py:190
  266.1 3.9 %collective-permute-start.7 = (bf16[4,128,224]{2,1,0:T(8,128)(2,1)S(1)}, bf16[4,128,224]{2,1,0:T(8,128)(2,1)S(1)}, u32[]{:S(2)}, u32[]{:S(2)}) collective-permute-start(bf16[4,128,224]{2,1,0:T(8,128)(2,1)S(1)} %copy-done), channel_id=1, source_target_pairs={{0,8},{1,9},{2,10},{3,11},{4,12},{5,13},{6,14},{7,15},{8,16},{9,17... | collective-permute-start | bytes 688136 | tf_op jit(solution)/shard_map/ppermute | solution.py:193
  270.0 3.7 %collective-permute-start.8 = (bf16[4,128,224]{2,1,0:T(8,128)(2,1)S(1)}, bf16[4,128,224]{2,1,0:T(8,128)(2,1)S(1)}, u32[]{:S(2)}, u32[]{:S(2)}) collective-permute-start(bf16[4,128,224]{2,1,0:T(8,128)(2,1)S(1)} %copy-done), channel_id=1, source_target_pairs={{0,16},{1,17},{2,18},{3,19},{4,20},{5,21},{6,22},{7,23},{8,24},{9,... | collective-permute-start | bytes 688136 | tf_op jit(solution)/shard_map/ppermute | solution.py:193
  273.7 2.5 collective-permute-start.9
  276.3 6.9 %collective-permute-done.8.refs_2_ = bf16[4,128,224]{2,1,0:T(8,128)(2,1)S(1)} collective-permute-done((bf16[4,128,224]{2,1,0:T(8,128)(2,1)S(1)}, bf16[4,128,224]{2,1,0:T(8,128)(2,1)S(1)}, u32[]{:S(2)}, u32[]{:S(2)}) %collective-permute-start.8) | collective-permute-done | bytes 229408 | tf_op jit(solution)/shard_map/ppermute | solution.py:193
  285.1 5.9 %collective-permute-start.14 = (bf16[4,64,512]{2,1,0:T(8,128)(2,1)S(1)}, bf16[4,64,512]{2,1,0:T(8,128)(2,1)S(1)}, u32[]{:S(2)}, u32[]{:S(2)}) collective-permute-start(bf16[4,64,512]{2,1,0:T(8,128)(2,1)S(1)} %slice.49), channel_id=1, source_target_pairs={{0,448},{1,65},{2,450},{3,67},{4,452},{5,69},{6,454},{7,71},{8,456... | collective-permute-start | bytes 786440 | tf_op jit(solution)/shard_map/ppermute | solution.py:190
  291.0 5.7 %collective-permute-done.14 = bf16[4,64,512]{2,1,0:T(8,128)(2,1)S(1)} collective-permute-done((bf16[4,64,512]{2,1,0:T(8,128)(2,1)S(1)}, bf16[4,64,512]{2,1,0:T(8,128)(2,1)S(1)}, u32[]{:S(2)}, u32[]{:S(2)}) %collective-permute-start.14) | collective-permute-done | bytes 262176 | tf_op jit(solution)/shard_map/ppermute | solution.py:190
  296.8 4.5 %collective-permute-start.15 = (bf16[4,32,512]{2,1,0:T(8,128)(2,1)S(1)}, bf16[4,32,512]{2,1,0:T(8,128)(2,1)S(1)}, u32[]{:S(2)}, u32[]{:S(2)}) collective-permute-start(bf16[4,32,512]{2,1,0:T(8,128)(2,1)S(1)} %slice.50), channel_id=1, source_target_pairs={{0,384},{1,129},{2,386},{3,131},{4,388},{5,133},{6,390},{7,135},{8... | collective-permute-start | bytes 393224 | tf_op jit(solution)/shard_map/ppermute | solution.py:190
  301.3 8.3 %collective-permute-done.15 = bf16[4,32,512]{2,1,0:T(8,128)(2,1)S(1)} collective-permute-done((bf16[4,32,512]{2,1,0:T(8,128)(2,1)S(1)}, bf16[4,32,512]{2,1,0:T(8,128)(2,1)S(1)}, u32[]{:S(2)}, u32[]{:S(2)}) %collective-permute-start.15) | collective-permute-done | bytes 131104 | tf_op jit(solution)/shard_map/ppermute | solution.py:190
  309.6 1.1 broadcast_in_dim.71
  310.7 5.9 %all-to-all-start.4 = ((bf16[32,32,512]{2,1,0:T(8,128)(2,1)}), bf16[32,32,512]{2,1,0:T(8,128)(2,1)S(1)}, u32[]{:S(2)}, u32[]{:S(2)}) async-start(bf16[32,32,512]{2,1,0:T(8,128)(2,1)} %bitcast.12), calls=%async_computation.4 | async-start | bytes 2097152 | tf_op jit(solution)/shard_map/all_to_all | solution.py:266
  317.9 2.2 copy.33
  320.2 1.3 copy.34
  321.4 12.3 %all-to-all-done.4 = bf16[32,32,512]{2,1,0:T(8,128)(2,1)S(1)} async-done(((bf16[32,32,512]{2,1,0:T(8,128)(2,1)}), bf16[32,32,512]{2,1,0:T(8,128)(2,1)S(1)}, u32[]{:S(2)}, u32[]{:S(2)}) %all-to-all-start.4) | async-done | bytes 1048608 | tf_op jit(solution)/shard_map/all_to_all | solution.py:266
  334.5 1.3 convolution_convert_fusion
  (52 shorter events, 11.1 us)
Async XLA Ops:
  2.0 16.6 %copy-start.4 = (f32[8,224,128]{2,1,0:T(8,128)S(1)}, f32[8,224,128]{2,1,0:T(8,128)}, u32[]{:S(2)}) copy-start(f32[8,224,128]{2,1,0:T(8,128)} %param.13) | copy-start | bytes 2752516
  8.3 23.9 %all-to-all-start = ((bf16[8,448,128]{2,1,0:T(8,128)(2,1)}), bf16[8,448,128]{2,1,0:T(8,128)(2,1)S(1)}, u32[]{:S(2)}, u32[]{:S(2)}) async-start(bf16[8,448,128]{2,1,0:T(8,128)(2,1)} %pack.1), calls=%async_computation | async-start | bytes 1835008 | tf_op jit(solution)/shard_map/all_to_all | solution.py:220
  32.2 13.0 %all-to-all-start.2 = ((bf16[8,224,128]{2,1,0:T(8,128)(2,1)}), bf16[8,224,128]{2,1,0:T(8,128)(2,1)S(1)}, u32[]{:S(2)}, u32[]{:S(2)}) async-start(bf16[8,224,128]{2,1,0:T(8,128)(2,1)} %convert_element_type.51), calls=%async_computation.2 | async-start | bytes 917504 | tf_op jit(solution)/shard_map/all_to_all | solution.py:214
  37.9 21.2 %copy-start.5 = (s32[128,2]{0,1:T(2,128)S(1)}, s32[128,2]{0,1:T(2,128)}, u32[]{:S(2)}) copy-start(s32[128,2]{0,1:T(2,128)} %param.8) | copy-start | bytes 3076
  37.9 21.5 %copy-start.1 = (bf16[128,2048]{1,0:T(8,128)(2,1)S(1)}, bf16[128,2048]{1,0:T(8,128)(2,1)}, u32[]{:S(2)}) copy-start(bf16[128,2048]{1,0:T(8,128)(2,1)} %param.7) | copy-start | bytes 1572868
  45.2 178.9 %all-to-all-start.1 = ((bf16[64,112,128]{2,1,0:T(8,128)(2,1)}), bf16[64,112,128]{2,1,0:T(8,128)(2,1)S(1)}, u32[]{:S(2)}, u32[]{:S(2)}) async-start(bf16[64,112,128]{2,1,0:T(8,128)(2,1)} %pad_maximum_fusion), calls=%async_computation.1 | async-start | bytes 3670016 | tf_op jit(solution)/shard_map/all_to_all | solution.py:222
  60.0 88.2 %collective-permute-start = (bf16[32,2048]{1,0:T(8,128)(2,1)S(1)}, bf16[32,2048]{1,0:T(8,128)(2,1)S(1)}, u32[]{:S(2)}, u32[]{:S(2)}) collective-permute-start(bf16[32,2048]{1,0:T(8,128)(2,1)S(1)} %convolution_convert_fusion.1), channel_id=1, source_target_pairs={{0,128},{1,385},{2,130},{3,387},{4,132},{5,389},{6,134},{7,391},{8... | collective-permute-start | bytes 393224 | tf_op jit(solution)/shard_map/ppermute | solution.py:190
  148.2 9.3 %collective-permute-start.1 = (bf16[64,2048]{1,0:T(8,128)(2,1)S(1)}, bf16[64,2048]{1,0:T(8,128)(2,1)S(1)}, u32[]{:S(2)}, u32[]{:S(2)}) collective-permute-start(bf16[64,2048]{1,0:T(8,128)(2,1)S(1)} %pad_maximum_fusion.4), channel_id=1, source_target_pairs={{0,64},{1,449},{2,66},{3,451},{4,68},{5,453},{6,70},{7,455},{8,72}... | collective-permute-start | bytes 786440 | tf_op jit(solution)/shard_map/ppermute | solution.py:190
  157.6 11.3 %collective-permute-start.2 = (bf16[128,2048]{1,0:T(8,128)(2,1)S(1)}, bf16[128,2048]{1,0:T(8,128)(2,1)S(1)}, u32[]{:S(2)}, u32[]{:S(2)}) collective-permute-start(bf16[128,2048]{1,0:T(8,128)(2,1)S(1)} %pad_maximum_fusion.3), channel_id=1, source_target_pairs={{0,32},{1,481},{2,34},{3,483},{4,36},{5,485},{6,38},{7,487},{8,40}... | collective-permute-start | bytes 1572872 | tf_op jit(solution)/shard_map/ppermute | solution.py:190
  169.9 24.3 %collective-permute-start.3 = (bf16[256,2048]{1,0:T(8,128)(2,1)}, bf16[256,2048]{1,0:T(8,128)(2,1)}, u32[]{:S(2)}, u32[]{:S(2)}) collective-permute-start(bf16[256,2048]{1,0:T(8,128)(2,1)} %pad_maximum_fusion.2), channel_id=1, source_target_pairs={{0,8},{1,9},{2,10},{3,11},{4,12},{5,13},{6,14},{7,15},{8,16},{9,17... | collective-permute-start | bytes 3145736 | tf_op jit(solution)/shard_map/ppermute | solution.py:193
  172.9 45.1 %collective-permute-start.4 = (bf16[256,2048]{1,0:T(8,128)(2,1)}, bf16[256,2048]{1,0:T(8,128)(2,1)}, u32[]{:S(2)}, u32[]{:S(2)}) collective-permute-start(bf16[256,2048]{1,0:T(8,128)(2,1)} %pad_maximum_fusion.2), channel_id=1, source_target_pairs={{0,16},{1,17},{2,18},{3,19},{4,20},{5,21},{6,22},{7,23},{8,24},{9,... | collective-permute-start | bytes 3145736 | tf_op jit(solution)/shard_map/ppermute | solution.py:193
  179.2 58.5 %collective-permute-start.6 = (bf16[224,1024]{1,0:T(8,128)(2,1)}, bf16[224,1024]{1,0:T(8,128)(2,1)}, u32[]{:S(2)}, u32[]{:S(2)}) collective-permute-start(bf16[224,1024]{1,0:T(8,128)(2,1)} %copy_bitcast_fusion), channel_id=1, source_target_pairs={{0,256},{1,257},{2,258},{3,259},{4,260},{5,261},{6,262},{7,263},{8... | collective-permute-start | bytes 1376264 | tf_op jit(solution)/shard_map/ppermute | solution.py:217
  187.2 35.9 %collective-permute-start.5 = (bf16[256,2048]{1,0:T(8,128)(2,1)}, bf16[256,2048]{1,0:T(8,128)(2,1)S(1)}, u32[]{:S(2)}, u32[]{:S(2)}) collective-permute-start(bf16[256,2048]{1,0:T(8,128)(2,1)} %pad_maximum_fusion.2), channel_id=1, source_target_pairs={{0,24},{1,25},{2,26},{3,27},{4,28},{5,29},{6,30},{7,31},{8,0},{9,1... | collective-permute-start | bytes 3145736 | tf_op jit(solution)/shard_map/ppermute | solution.py:193
  224.1 1.2 copy-start.2
  233.0 28.3 %all-to-all-start.3 = ((bf16[4,4,128,256]{3,2,1,0:T(8,128)(2,1)}), bf16[4,4,128,256]{3,2,1,0:T(8,128)(2,1)S(1)}, u32[]{:S(2)}, u32[]{:S(2)}) async-start(bf16[4,4,128,256]{3,2,1,0:T(8,128)(2,1)} %get-tuple-element.15), calls=%async_computation.3 | async-start | bytes 2097152 | tf_op jit(solution)/shard_map/all_to_all | solution.py:250
  238.8 27.3 %copy-start = (bf16[4,128,224]{2,1,0:T(8,128)(2,1)S(1)}, bf16[4,128,224]{2,1,0:T(8,128)(2,1)}, u32[]{:S(2)}) copy-start(bf16[4,128,224]{2,1,0:T(8,128)(2,1)} %get-tuple-element.14.refs_0_) | copy-start | bytes 688132
  239.4 16.6 %collective-permute-start.10 = (bf16[224,512]{1,0:T(8,128)(2,1)S(1)}, bf16[224,512]{1,0:T(8,128)(2,1)S(1)}, u32[]{:S(2)}, u32[]{:S(2)}) collective-permute-start(bf16[224,512]{1,0:T(8,128)(2,1)S(1)} %get-tuple-element.34), channel_id=1, source_target_pairs={{0,8},{1,9},{2,10},{3,11},{4,12},{5,13},{6,14},{7,15},{8,16},{9,17... | collective-permute-start | bytes 688136 | tf_op jit(solution)/shard_map/ppermute | solution.py:193
  242.8 18.5 %collective-permute-start.11 = (bf16[224,512]{1,0:T(8,128)(2,1)S(1)}, bf16[224,512]{1,0:T(8,128)(2,1)S(1)}, u32[]{:S(2)}, u32[]{:S(2)}) collective-permute-start(bf16[224,512]{1,0:T(8,128)(2,1)S(1)} %get-tuple-element.35), channel_id=1, source_target_pairs={{0,16},{1,17},{2,18},{3,19},{4,20},{5,21},{6,22},{7,23},{8,24},{9,... | collective-permute-start | bytes 688136 | tf_op jit(solution)/shard_map/ppermute | solution.py:193
  247.1 14.2 %collective-permute-start.12 = (bf16[224,512]{1,0:T(8,128)(2,1)S(1)}, bf16[224,512]{1,0:T(8,128)(2,1)S(1)}, u32[]{:S(2)}, u32[]{:S(2)}) collective-permute-start(bf16[224,512]{1,0:T(8,128)(2,1)S(1)} %get-tuple-element.32), channel_id=1, source_target_pairs={{0,24},{1,25},{2,26},{3,27},{4,28},{5,29},{6,30},{7,31},{8,0},{9,1... | collective-permute-start | bytes 688136 | tf_op jit(solution)/shard_map/ppermute | solution.py:193
  262.0 22.8 %collective-permute-start.13 = (bf16[4,128,512]{2,1,0:T(8,128)(2,1)S(1)}, bf16[4,128,512]{2,1,0:T(8,128)(2,1)S(1)}, u32[]{:S(2)}, u32[]{:S(2)}) collective-permute-start(bf16[4,128,512]{2,1,0:T(8,128)(2,1)S(1)} %partial_out.3), channel_id=1, source_target_pairs={{0,480},{1,33},{2,482},{3,35},{4,484},{5,37},{6,486},{7,39},{8,488... | collective-permute-start | bytes 1572872 | tf_op jit(solution)/shard_map/ppermute | solution.py:190
  266.1 10.1 %collective-permute-start.7 = (bf16[4,128,224]{2,1,0:T(8,128)(2,1)S(1)}, bf16[4,128,224]{2,1,0:T(8,128)(2,1)S(1)}, u32[]{:S(2)}, u32[]{:S(2)}) collective-permute-start(bf16[4,128,224]{2,1,0:T(8,128)(2,1)S(1)} %copy-done), channel_id=1, source_target_pairs={{0,8},{1,9},{2,10},{3,11},{4,12},{5,13},{6,14},{7,15},{8,16},{9,17... | collective-permute-start | bytes 688136 | tf_op jit(solution)/shard_map/ppermute | solution.py:193
  270.0 13.1 %collective-permute-start.8 = (bf16[4,128,224]{2,1,0:T(8,128)(2,1)S(1)}, bf16[4,128,224]{2,1,0:T(8,128)(2,1)S(1)}, u32[]{:S(2)}, u32[]{:S(2)}) collective-permute-start(bf16[4,128,224]{2,1,0:T(8,128)(2,1)S(1)} %copy-done), channel_id=1, source_target_pairs={{0,16},{1,17},{2,18},{3,19},{4,20},{5,21},{6,22},{7,23},{8,24},{9,... | collective-permute-start | bytes 688136 | tf_op jit(solution)/shard_map/ppermute | solution.py:193
  273.7 10.4 %collective-permute-start.9 = (bf16[4,128,224]{2,1,0:T(8,128)(2,1)S(1)}, bf16[4,128,224]{2,1,0:T(8,128)(2,1)S(1)}, u32[]{:S(2)}, u32[]{:S(2)}) collective-permute-start(bf16[4,128,224]{2,1,0:T(8,128)(2,1)S(1)} %copy-done), channel_id=1, source_target_pairs={{0,24},{1,25},{2,26},{3,27},{4,28},{5,29},{6,30},{7,31},{8,0},{9,1... | collective-permute-start | bytes 688136 | tf_op jit(solution)/shard_map/ppermute | solution.py:193
  285.1 11.5 %collective-permute-start.14 = (bf16[4,64,512]{2,1,0:T(8,128)(2,1)S(1)}, bf16[4,64,512]{2,1,0:T(8,128)(2,1)S(1)}, u32[]{:S(2)}, u32[]{:S(2)}) collective-permute-start(bf16[4,64,512]{2,1,0:T(8,128)(2,1)S(1)} %slice.49), channel_id=1, source_target_pairs={{0,448},{1,65},{2,450},{3,67},{4,452},{5,69},{6,454},{7,71},{8,456... | collective-permute-start | bytes 786440 | tf_op jit(solution)/shard_map/ppermute | solution.py:190
  296.7 19.9 %copy-start.6 = (f32[128,2]{0,1:T(2,128)S(1)}, f32[128,2]{0,1:T(2,128)}, u32[]{:S(2)}) copy-start(f32[128,2]{0,1:T(2,128)} %param.9) | copy-start | bytes 3076
  296.8 12.8 %collective-permute-start.15 = (bf16[4,32,512]{2,1,0:T(8,128)(2,1)S(1)}, bf16[4,32,512]{2,1,0:T(8,128)(2,1)S(1)}, u32[]{:S(2)}, u32[]{:S(2)}) collective-permute-start(bf16[4,32,512]{2,1,0:T(8,128)(2,1)S(1)} %slice.50), channel_id=1, source_target_pairs={{0,384},{1,129},{2,386},{3,131},{4,388},{5,133},{6,390},{7,135},{8... | collective-permute-start | bytes 393224 | tf_op jit(solution)/shard_map/ppermute | solution.py:190
  310.7 23.0 %all-to-all-start.4 = ((bf16[32,32,512]{2,1,0:T(8,128)(2,1)}), bf16[32,32,512]{2,1,0:T(8,128)(2,1)S(1)}, u32[]{:S(2)}, u32[]{:S(2)}) async-start(bf16[32,32,512]{2,1,0:T(8,128)(2,1)} %bitcast.12), calls=%async_computation.4 | async-start | bytes 2097152 | tf_op jit(solution)/shard_map/all_to_all | solution.py:266
  316.7 3.5 %copy-start.3 = (bf16[1,2048,224]{2,1,0:T(8,128)(2,1)S(1)}, bf16[1,2048,224]{2,1,0:T(8,128)(2,1)}, u32[]{:S(2)}) copy-start(bf16[1,2048,224]{2,1,0:T(8,128)(2,1)} %get-tuple-element.29) | copy-start | bytes 2752516
where the time goes:
time: 340 us; the launch traced here: 336 us
  waiting for transfers between devices  187 us (55%)
  starting transfers between devices  106 us (31%)
  local copies, waits for them, and re-layouts  16.8 us (5%)
  Pallas kernels  15.4 us (5%)
  other arithmetic  8.37 us (2%)
    ppermute x6, waiting for transfers between devices, along_z(): return lax.ppermute(x, ALL, pairs)  110 us
    ppermute x9, waiting for transfers between devices, along_y(): lax.ppermute(x, ALL, permutation(sizes, lambda z, y, t: (z, y + hops)))  44.8 us
    ppermute x9, starting transfers between devices, along_y(): lax.ppermute(x, ALL, permutation(sizes, lambda z, y, t: (z, y + hops)))  31.2 us
    ppermute x6, starting transfers between devices, along_z(): return lax.ppermute(x, ALL, pairs)  27.7 us
    all_to_all x1, starting transfers between devices, local(): tiles = lax.all_to_all(tiles, GR_FS, 0, 0, tiled=True)  13.9 us
    all_to_all x1, waiting for transfers between devices, local(): lax.all_to_all(tiles, 'tp', 0, 0, tiled=True).reshape(-1, 112, LANES)  12.8 us
    all_to_all x1, waiting for transfers between devices, local(): lax.all_to_all(block.reshape(-1, *block.shape[2:]), ('fs_1', 'tp'), 0, 0,...  12.3 us
    all_to_all x1, starting transfers between devices, local(): lax.all_to_all(tiles, 'tp', 0, 0, tiled=True).reshape(-1, 112, LANES)  10.3 us
  transfers between devices with their start and end apart: 21, of which 15 were waited for; matrix products, arithmetic and copies ran while one was open for 6% of the time, Pallas kernels for 3%

commit v1 on v0

--- a/solution.py
+++ b/solution.py
@@ -64,12 +64,12 @@
     def _():
         lane = lax.broadcasted_iota(jnp.int32, (16, LANES), 1)
 
-        def unpack(s, carry):
-            rows = pl.ds(pl.multiple_of(32 * s, 32), 32)
+        for s in range(tiles_ref.shape[0]):
+            rows = pl.ds(32 * s, 32)
             gate_ref[0, rows, :LANES] = tiles_ref[s, 0:32, :]
             up_ref[0, rows, :LANES] = tiles_ref[s, 32:64, :]
             gate_ref[0, rows, LANES:] = tiles_ref[s, 64:96, :96]
-            up_ref[0, pl.ds(pl.multiple_of(32 * s, 16), 16), LANES:] = tiles_ref[s, 96:112, :96]
+            up_ref[0, pl.ds(32 * s, 16), LANES:] = tiles_ref[s, 96:112, :96]
             parts = [
                 pltpu.roll(
                     tiles_ref[s, 64 + 16 * q : 80 + 16 * q, :].astype(jnp.float32), 32 * q + 32, 1
@@ -77,11 +77,7 @@
                 for q in range(3)
             ]
             last = jnp.where(lane < 32, parts[0], jnp.where(lane < 64, parts[1], parts[2]))
-            rest = pl.ds(pl.multiple_of(32 * s + 16, 16), 16)
-            up_ref[0, rest, LANES:] = last[:, :96].astype(jnp.bfloat16)
-            return carry
-
-        lax.fori_loop(0, tiles_ref.shape[0], unpack, 0, unroll=4)
+            up_ref[0, pl.ds(32 * s + 16, 16), LANES:] = last[:, :96].astype(jnp.bfloat16)
 
     tokens = tokens_ref[...]
     gate = jnp.dot(tokens, gate_ref[0], preferred_element_type=jnp.float32)

time: 340 us -> 340 us (level)
  transfers between devices with their start and end apart: 21 -> 21, of which waited for: 15 -> 15; matrix products, arithmetic and copies ran while one was open for 6% -> 6% of each run, Pallas kernels for 3% -> 2%
where the time goes in v1:
time: 340 us; the launch traced here: 335 us
  waiting for transfers between devices  187 us (55%)
  starting transfers between devices  106 us (31%)
  local copies, waits for them, and re-layouts  16.8 us (5%)
  Pallas kernels  14.6 us (4%)
  other arithmetic  8.37 us (2%)
    ppermute x6, waiting for transfers between devices, along_z(): return lax.ppermute(x, ALL, pairs)  110 us
    ppermute x9, waiting for transfers between devices, along_y(): lax.ppermute(x, ALL, permutation(sizes, lambda z, y, t: (z, y + hops)))  44.8 us
    ppermute x9, starting transfers between devices, along_y(): lax.ppermute(x, ALL, permutation(sizes, lambda z, y, t: (z, y + hops)))  31.1 us
    ppermute x6, starting transfers between devices, along_z(): return lax.ppermute(x, ALL, pairs)  27.6 us
    all_to_all x1, starting transfers between devices, local(): tiles = lax.all_to_all(tiles, GR_FS, 0, 0, tiled=True)  13.9 us
    all_to_all x1, waiting for transfers between devices, local(): lax.all_to_all(tiles, 'tp', 0, 0, tiled=True).reshape(-1, 112, LANES)  12.8 us
    all_to_all x1, waiting for transfers between devices, local(): lax.all_to_all(block.reshape(-1, *block.shape[2:]), ('fs_1', 'tp'), 0, 0,...  12.3 us
    all_to_all x1, starting transfers between devices, local(): lax.all_to_all(tiles, 'tp', 0, 0, tiled=True).reshape(-1, 112, LANES)  10.3 us
  transfers between devices with their start and end apart: 21, of which 15 were waited for; matrix products, arithmetic and copies ran while one was open for 6% of the time, Pallas kernels for 2%

profile of v1, /device:TPU:1, one launch (start us, length us, event | category | flops | bytes accessed | tf_op | source)
XLA Modules:
  0.0 335.2 jit_solution(17084732825448661328)
XLA Ops:
  0.6 1.3 copy.30.gain_ref
  2.0 6.3 %pack.1 = bf16[8,448,128]{2,1,0:T(8,128)(2,1)} custom-call(f32[8,32,896]{2,1,0:T(8,128)} %gate_ref.1, f32[8,32,896]{2,1,0:T(8,128)} %up_ref.1, f32[32,1]{1,0:T(8,128)} %copy.30.gain_ref), custom_call_target="tpu_custom_call" | custom-call | flops 4000000 | bytes 2800000 | tf_op jit(solution)/shard_map/pack/pallas_call | solution.py:46
  8.3 10.3 %all-to-all-start = ((bf16[8,448,128]{2,1,0:T(8,128)(2,1)}), bf16[8,448,128]{2,1,0:T(8,128)(2,1)S(1)}, u32[]{:S(2)}, u32[]{:S(2)}) async-start(bf16[8,448,128]{2,1,0:T(8,128)(2,1)} %pack.1), calls=%async_computation | async-start | bytes 1835008 | tf_op jit(solution)/shard_map/all_to_all | solution.py:216
  19.4 12.8 %all-to-all-done = bf16[8,448,128]{2,1,0:T(8,128)(2,1)S(1)} async-done(((bf16[8,448,128]{2,1,0:T(8,128)(2,1)}), bf16[8,448,128]{2,1,0:T(8,128)(2,1)S(1)}, u32[]{:S(2)}, u32[]{:S(2)}) %all-to-all-start) | async-done | bytes 917536 | tf_op jit(solution)/shard_map/all_to_all | solution.py:216
  32.2 4.3 %all-to-all-start.2 = ((bf16[8,224,128]{2,1,0:T(8,128)(2,1)}), bf16[8,224,128]{2,1,0:T(8,128)(2,1)S(1)}, u32[]{:S(2)}, u32[]{:S(2)}) async-start(bf16[8,224,128]{2,1,0:T(8,128)(2,1)} %convert_element_type.51), calls=%async_computation.2 | async-start | bytes 917504 | tf_op jit(solution)/shard_map/all_to_all | solution.py:210
  36.5 1.4 pad_maximum_fusion
  37.9 7.3 %all-to-all-done.2 = bf16[8,224,128]{2,1,0:T(8,128)(2,1)S(1)} async-done(((bf16[8,224,128]{2,1,0:T(8,128)(2,1)}), bf16[8,224,128]{2,1,0:T(8,128)(2,1)S(1)}, u32[]{:S(2)}, u32[]{:S(2)}) %all-to-all-start.2) | async-done | bytes 458784 | tf_op jit(solution)/shard_map/all_to_all | solution.py:210
  45.2 13.9 %all-to-all-start.1 = ((bf16[64,112,128]{2,1,0:T(8,128)(2,1)}), bf16[64,112,128]{2,1,0:T(8,128)(2,1)S(1)}, u32[]{:S(2)}, u32[]{:S(2)}) async-start(bf16[64,112,128]{2,1,0:T(8,128)(2,1)} %pad_maximum_fusion), calls=%async_computation.1 | async-start | bytes 3670016 | tf_op jit(solution)/shard_map/all_to_all | solution.py:218
  60.0 7.0 %collective-permute-start = (bf16[32,2048]{1,0:T(8,128)(2,1)S(1)}, bf16[32,2048]{1,0:T(8,128)(2,1)S(1)}, u32[]{:S(2)}, u32[]{:S(2)}) collective-permute-start(bf16[32,2048]{1,0:T(8,128)(2,1)S(1)} %convolution_convert_fusion.1), channel_id=1, source_target_pairs={{0,128},{1,385},{2,130},{3,387},{4,132},{5,389},{6,134},{7,391},{8... | collective-permute-start | bytes 393224 | tf_op jit(solution)/shard_map/ppermute | solution.py:186
  67.0 81.2 %collective-permute-done = bf16[32,2048]{1,0:T(8,128)(2,1)S(1)} collective-permute-done((bf16[32,2048]{1,0:T(8,128)(2,1)S(1)}, bf16[32,2048]{1,0:T(8,128)(2,1)S(1)}, u32[]{:S(2)}, u32[]{:S(2)}) %collective-permute-start) | collective-permute-done | bytes 131104 | tf_op jit(solution)/shard_map/ppermute | solution.py:186
  148.2 1.9 collective-permute-start.1
  150.2 7.4 %collective-permute-done.1 = bf16[64,2048]{1,0:T(8,128)(2,1)S(1)} collective-permute-done((bf16[64,2048]{1,0:T(8,128)(2,1)S(1)}, bf16[64,2048]{1,0:T(8,128)(2,1)S(1)}, u32[]{:S(2)}, u32[]{:S(2)}) %collective-permute-start.1) | collective-permute-done | bytes 262176 | tf_op jit(solution)/shard_map/ppermute | solution.py:186
  157.6 4.2 %collective-permute-start.2 = (bf16[128,2048]{1,0:T(8,128)(2,1)S(1)}, bf16[128,2048]{1,0:T(8,128)(2,1)S(1)}, u32[]{:S(2)}, u32[]{:S(2)}) collective-permute-start(bf16[128,2048]{1,0:T(8,128)(2,1)S(1)} %pad_maximum_fusion.3), channel_id=1, source_target_pairs={{0,32},{1,481},{2,34},{3,483},{4,36},{5,485},{6,38},{7,487},{8,40}... | collective-permute-start | bytes 1572872 | tf_op jit(solution)/shard_map/ppermute | solution.py:186
  161.8 7.1 %collective-permute-done.2 = bf16[128,2048]{1,0:T(8,128)(2,1)S(1)} collective-permute-done((bf16[128,2048]{1,0:T(8,128)(2,1)S(1)}, bf16[128,2048]{1,0:T(8,128)(2,1)S(1)}, u32[]{:S(2)}, u32[]{:S(2)}) %collective-permute-start.2) | collective-permute-done | bytes 524320 | tf_op jit(solution)/shard_map/ppermute | solution.py:186
  169.9 3.0 collective-permute-start.3
  172.9 5.3 %collective-permute-start.4 = (bf16[256,2048]{1,0:T(8,128)(2,1)}, bf16[256,2048]{1,0:T(8,128)(2,1)}, u32[]{:S(2)}, u32[]{:S(2)}) collective-permute-start(bf16[256,2048]{1,0:T(8,128)(2,1)} %pad_maximum_fusion.2), channel_id=1, source_target_pairs={{0,16},{1,17},{2,18},{3,19},{4,20},{5,21},{6,22},{7,23},{8,24},{9,... | collective-permute-start | bytes 3145736 | tf_op jit(solution)/shard_map/ppermute | solution.py:189
  179.2 8.0 %collective-permute-start.6 = (bf16[224,1024]{1,0:T(8,128)(2,1)}, bf16[224,1024]{1,0:T(8,128)(2,1)}, u32[]{:S(2)}, u32[]{:S(2)}) collective-permute-start(bf16[224,1024]{1,0:T(8,128)(2,1)} %copy_bitcast_fusion), channel_id=1, source_target_pairs={{0,256},{1,257},{2,258},{3,259},{4,260},{5,261},{6,262},{7,263},{8... | collective-permute-start | bytes 1376264 | tf_op jit(solution)/shard_map/ppermute | solution.py:213
  187.2 1.9 collective-permute-start.5
  189.1 2.5 broadcast_in_dim.64
  192.6 1.6 collective-permute-done.3
  194.2 2.3 bitcast_dynamic-update-slice_fusion.2
  196.5 21.5 %collective-permute-done.4 = bf16[256,2048]{1,0:T(8,128)(2,1)} collective-permute-done((bf16[256,2048]{1,0:T(8,128)(2,1)}, bf16[256,2048]{1,0:T(8,128)(2,1)}, u32[]{:S(2)}, u32[]{:S(2)}) %collective-permute-start.4) | collective-permute-done | bytes 1048608 | tf_op jit(solution)/shard_map/ppermute | solution.py:189
  218.0 2.3 bitcast_dynamic-update-slice_fusion.1
  220.4 2.7 collective-permute-done.5
  224.1 1.2 copy-done.2
  225.3 6.9 %hidden_units.1 = (bf16[1,2048,224]{2,1,0:T(8,128)(2,1)}, bf16[1,2048,224]{2,1,0:T(8,128)(2,1)}, bf16[4,128,224]{2,1,0:T(8,128)(2,1)}, bf16[4,4,128,256]{3,2,1,0:T(8,128)(2,1)}) custom-call(bf16[64,112,128]{2,1,0:T(8,128)(2,1)} %copy-done.2, bf16[1024,2048]{1,0:T(8,128)(2,1)} %bitcast.7.tokens_ref), custom_call_target="tpu_custom_call" | custom-call | flops 1900000000 | bytes 8500000 | tf_op jit(solution)/shard_map/hidden_units/pallas_call | solution.py:99
  232.2 4.6 %all-to-all-start.3 = ((bf16[4,4,128,256]{3,2,1,0:T(8,128)(2,1)}), bf16[4,4,128,256]{3,2,1,0:T(8,128)(2,1)S(1)}, u32[]{:S(2)}, u32[]{:S(2)}) async-start(bf16[4,4,128,256]{3,2,1,0:T(8,128)(2,1)} %get-tuple-element.15), calls=%async_computation.3 | async-start | bytes 2097152 | tf_op jit(solution)/shard_map/all_to_all | solution.py:246
  236.8 1.2 broadcast_select_fusion.1
  238.6 3.4 %collective-permute-start.10 = (bf16[224,512]{1,0:T(8,128)(2,1)S(1)}, bf16[224,512]{1,0:T(8,128)(2,1)S(1)}, u32[]{:S(2)}, u32[]{:S(2)}) collective-permute-start(bf16[224,512]{1,0:T(8,128)(2,1)S(1)} %get-tuple-element.34), channel_id=1, source_target_pairs={{0,8},{1,9},{2,10},{3,11},{4,12},{5,13},{6,14},{7,15},{8,16},{9,17... | collective-permute-start | bytes 688136 | tf_op jit(solution)/shard_map/ppermute | solution.py:189
  242.0 4.3 %collective-permute-start.11 = (bf16[224,512]{1,0:T(8,128)(2,1)S(1)}, bf16[224,512]{1,0:T(8,128)(2,1)S(1)}, u32[]{:S(2)}, u32[]{:S(2)}) collective-permute-start(bf16[224,512]{1,0:T(8,128)(2,1)S(1)} %get-tuple-element.35), channel_id=1, source_target_pairs={{0,16},{1,17},{2,18},{3,19},{4,20},{5,21},{6,22},{7,23},{8,24},{9,... | collective-permute-start | bytes 688136 | tf_op jit(solution)/shard_map/ppermute | solution.py:189
  246.3 3.1 collective-permute-start.12
  249.4 5.8 %collective-permute-done.10.refs_5_.refs_1_ = bf16[224,512]{1,0:T(8,128)(2,1)S(1)} collective-permute-done((bf16[224,512]{1,0:T(8,128)(2,1)S(1)}, bf16[224,512]{1,0:T(8,128)(2,1)S(1)}, u32[]{:S(2)}, u32[]{:S(2)}) %collective-permute-start.10) | collective-permute-done | bytes 229408 | tf_op jit(solution)/shard_map/ppermute | solution.py:189
  255.2 5.3 %collective-permute-done.11.refs_6_.refs_2_ = bf16[224,512]{1,0:T(8,128)(2,1)S(1)} collective-permute-done((bf16[224,512]{1,0:T(8,128)(2,1)S(1)}, bf16[224,512]{1,0:T(8,128)(2,1)S(1)}, u32[]{:S(2)}, u32[]{:S(2)}) %collective-permute-start.11) | collective-permute-done | bytes 229408 | tf_op jit(solution)/shard_map/ppermute | solution.py:189
  261.2 4.1 %collective-permute-start.13 = (bf16[4,128,512]{2,1,0:T(8,128)(2,1)S(1)}, bf16[4,128,512]{2,1,0:T(8,128)(2,1)S(1)}, u32[]{:S(2)}, u32[]{:S(2)}) collective-permute-start(bf16[4,128,512]{2,1,0:T(8,128)(2,1)S(1)} %partial_out.3), channel_id=1, source_target_pairs={{0,480},{1,33},{2,482},{3,35},{4,484},{5,37},{6,486},{7,39},{8,488... | collective-permute-start | bytes 1572872 | tf_op jit(solution)/shard_map/ppermute | solution.py:186
  265.3 3.9 %collective-permute-start.7 = (bf16[4,128,224]{2,1,0:T(8,128)(2,1)S(1)}, bf16[4,128,224]{2,1,0:T(8,128)(2,1)S(1)}, u32[]{:S(2)}, u32[]{:S(2)}) collective-permute-start(bf16[4,128,224]{2,1,0:T(8,128)(2,1)S(1)} %copy-done), channel_id=1, source_target_pairs={{0,8},{1,9},{2,10},{3,11},{4,12},{5,13},{6,14},{7,15},{8,16},{9,17... | collective-permute-start | bytes 688136 | tf_op jit(solution)/shard_map/ppermute | solution.py:189
  269.2 3.7 %collective-permute-start.8 = (bf16[4,128,224]{2,1,0:T(8,128)(2,1)S(1)}, bf16[4,128,224]{2,1,0:T(8,128)(2,1)S(1)}, u32[]{:S(2)}, u32[]{:S(2)}) collective-permute-start(bf16[4,128,224]{2,1,0:T(8,128)(2,1)S(1)} %copy-done), channel_id=1, source_target_pairs={{0,16},{1,17},{2,18},{3,19},{4,20},{5,21},{6,22},{7,23},{8,24},{9,... | collective-permute-start | bytes 688136 | tf_op jit(solution)/shard_map/ppermute | solution.py:189
  272.9 2.5 collective-permute-start.9
  275.4 6.9 %collective-permute-done.8.refs_2_ = bf16[4,128,224]{2,1,0:T(8,128)(2,1)S(1)} collective-permute-done((bf16[4,128,224]{2,1,0:T(8,128)(2,1)S(1)}, bf16[4,128,224]{2,1,0:T(8,128)(2,1)S(1)}, u32[]{:S(2)}, u32[]{:S(2)}) %collective-permute-start.8) | collective-permute-done | bytes 229408 | tf_op jit(solution)/shard_map/ppermute | solution.py:189
  284.3 5.8 %collective-permute-start.14 = (bf16[4,64,512]{2,1,0:T(8,128)(2,1)S(1)}, bf16[4,64,512]{2,1,0:T(8,128)(2,1)S(1)}, u32[]{:S(2)}, u32[]{:S(2)}) collective-permute-start(bf16[4,64,512]{2,1,0:T(8,128)(2,1)S(1)} %slice.49), channel_id=1, source_target_pairs={{0,448},{1,65},{2,450},{3,67},{4,452},{5,69},{6,454},{7,71},{8,456... | collective-permute-start | bytes 786440 | tf_op jit(solution)/shard_map/ppermute | solution.py:186
  290.1 5.7 %collective-permute-done.14 = bf16[4,64,512]{2,1,0:T(8,128)(2,1)S(1)} collective-permute-done((bf16[4,64,512]{2,1,0:T(8,128)(2,1)S(1)}, bf16[4,64,512]{2,1,0:T(8,128)(2,1)S(1)}, u32[]{:S(2)}, u32[]{:S(2)}) %collective-permute-start.14) | collective-permute-done | bytes 262176 | tf_op jit(solution)/shard_map/ppermute | solution.py:186
  296.0 4.5 %collective-permute-start.15 = (bf16[4,32,512]{2,1,0:T(8,128)(2,1)S(1)}, bf16[4,32,512]{2,1,0:T(8,128)(2,1)S(1)}, u32[]{:S(2)}, u32[]{:S(2)}) collective-permute-start(bf16[4,32,512]{2,1,0:T(8,128)(2,1)S(1)} %slice.50), channel_id=1, source_target_pairs={{0,384},{1,129},{2,386},{3,131},{4,388},{5,133},{6,390},{7,135},{8... | collective-permute-start | bytes 393224 | tf_op jit(solution)/shard_map/ppermute | solution.py:186
  300.5 8.3 %collective-permute-done.15 = bf16[4,32,512]{2,1,0:T(8,128)(2,1)S(1)} collective-permute-done((bf16[4,32,512]{2,1,0:T(8,128)(2,1)S(1)}, bf16[4,32,512]{2,1,0:T(8,128)(2,1)S(1)}, u32[]{:S(2)}, u32[]{:S(2)}) %collective-permute-start.15) | collective-permute-done | bytes 131104 | tf_op jit(solution)/shard_map/ppermute | solution.py:186
  308.8 1.1 broadcast_in_dim.71
  309.9 6.1 %all-to-all-start.4 = ((bf16[32,32,512]{2,1,0:T(8,128)(2,1)}), bf16[32,32,512]{2,1,0:T(8,128)(2,1)S(1)}, u32[]{:S(2)}, u32[]{:S(2)}) async-start(bf16[32,32,512]{2,1,0:T(8,128)(2,1)} %bitcast.12), calls=%async_computation.4 | async-start | bytes 2097152 | tf_op jit(solution)/shard_map/all_to_all | solution.py:262
  317.3 2.2 copy.33
  319.6 1.3 copy.34
  320.8 12.3 %all-to-all-done.4 = bf16[32,32,512]{2,1,0:T(8,128)(2,1)S(1)} async-done(((bf16[32,32,512]{2,1,0:T(8,128)(2,1)}), bf16[32,32,512]{2,1,0:T(8,128)(2,1)S(1)}, u32[]{:S(2)}, u32[]{:S(2)}) %all-to-all-start.4) | async-done | bytes 1048608 | tf_op jit(solution)/shard_map/all_to_all | solution.py:262
  333.9 1.3 convolution_convert_fusion
  (52 shorter events, 11.0 us)
Async XLA Ops:
  2.0 16.6 %copy-start.4 = (f32[8,224,128]{2,1,0:T(8,128)S(1)}, f32[8,224,128]{2,1,0:T(8,128)}, u32[]{:S(2)}) copy-start(f32[8,224,128]{2,1,0:T(8,128)} %param.13) | copy-start | bytes 2752516
  8.3 23.9 %all-to-all-start = ((bf16[8,448,128]{2,1,0:T(8,128)(2,1)}), bf16[8,448,128]{2,1,0:T(8,128)(2,1)S(1)}, u32[]{:S(2)}, u32[]{:S(2)}) async-start(bf16[8,448,128]{2,1,0:T(8,128)(2,1)} %pack.1), calls=%async_computation | async-start | bytes 1835008 | tf_op jit(solution)/shard_map/all_to_all | solution.py:216
  32.2 13.0 %all-to-all-start.2 = ((bf16[8,224,128]{2,1,0:T(8,128)(2,1)}), bf16[8,224,128]{2,1,0:T(8,128)(2,1)S(1)}, u32[]{:S(2)}, u32[]{:S(2)}) async-start(bf16[8,224,128]{2,1,0:T(8,128)(2,1)} %convert_element_type.51), calls=%async_computation.2 | async-start | bytes 917504 | tf_op jit(solution)/shard_map/all_to_all | solution.py:210
  37.9 21.2 %copy-start.5 = (s32[128,2]{0,1:T(2,128)S(1)}, s32[128,2]{0,1:T(2,128)}, u32[]{:S(2)}) copy-start(s32[128,2]{0,1:T(2,128)} %param.8) | copy-start | bytes 3076
  37.9 21.5 %copy-start.1 = (bf16[128,2048]{1,0:T(8,128)(2,1)S(1)}, bf16[128,2048]{1,0:T(8,128)(2,1)}, u32[]{:S(2)}) copy-start(bf16[128,2048]{1,0:T(8,128)(2,1)} %param.7) | copy-start | bytes 1572868
  45.2 178.9 %all-to-all-start.1 = ((bf16[64,112,128]{2,1,0:T(8,128)(2,1)}), bf16[64,112,128]{2,1,0:T(8,128)(2,1)S(1)}, u32[]{:S(2)}, u32[]{:S(2)}) async-start(bf16[64,112,128]{2,1,0:T(8,128)(2,1)} %pad_maximum_fusion), calls=%async_computation.1 | async-start | bytes 3670016 | tf_op jit(solution)/shard_map/all_to_all | solution.py:218
  60.0 88.2 %collective-permute-start = (bf16[32,2048]{1,0:T(8,128)(2,1)S(1)}, bf16[32,2048]{1,0:T(8,128)(2,1)S(1)}, u32[]{:S(2)}, u32[]{:S(2)}) collective-permute-start(bf16[32,2048]{1,0:T(8,128)(2,1)S(1)} %convolution_convert_fusion.1), channel_id=1, source_target_pairs={{0,128},{1,385},{2,130},{3,387},{4,132},{5,389},{6,134},{7,391},{8... | collective-permute-start | bytes 393224 | tf_op jit(solution)/shard_map/ppermute | solution.py:186
  148.2 9.3 %collective-permute-start.1 = (bf16[64,2048]{1,0:T(8,128)(2,1)S(1)}, bf16[64,2048]{1,0:T(8,128)(2,1)S(1)}, u32[]{:S(2)}, u32[]{:S(2)}) collective-permute-start(bf16[64,2048]{1,0:T(8,128)(2,1)S(1)} %pad_maximum_fusion.4), channel_id=1, source_target_pairs={{0,64},{1,449},{2,66},{3,451},{4,68},{5,453},{6,70},{7,455},{8,72}... | collective-permute-start | bytes 786440 | tf_op jit(solution)/shard_map/ppermute | solution.py:186
  157.6 11.3 %collective-permute-start.2 = (bf16[128,2048]{1,0:T(8,128)(2,1)S(1)}, bf16[128,2048]{1,0:T(8,128)(2,1)S(1)}, u32[]{:S(2)}, u32[]{:S(2)}) collective-permute-start(bf16[128,2048]{1,0:T(8,128)(2,1)S(1)} %pad_maximum_fusion.3), channel_id=1, source_target_pairs={{0,32},{1,481},{2,34},{3,483},{4,36},{5,485},{6,38},{7,487},{8,40}... | collective-permute-start | bytes 1572872 | tf_op jit(solution)/shard_map/ppermute | solution.py:186
  169.9 24.3 %collective-permute-start.3 = (bf16[256,2048]{1,0:T(8,128)(2,1)}, bf16[256,2048]{1,0:T(8,128)(2,1)}, u32[]{:S(2)}, u32[]{:S(2)}) collective-permute-start(bf16[256,2048]{1,0:T(8,128)(2,1)} %pad_maximum_fusion.2), channel_id=1, source_target_pairs={{0,8},{1,9},{2,10},{3,11},{4,12},{5,13},{6,14},{7,15},{8,16},{9,17... | collective-permute-start | bytes 3145736 | tf_op jit(solution)/shard_map/ppermute | solution.py:189
  172.9 45.1 %collective-permute-start.4 = (bf16[256,2048]{1,0:T(8,128)(2,1)}, bf16[256,2048]{1,0:T(8,128)(2,1)}, u32[]{:S(2)}, u32[]{:S(2)}) collective-permute-start(bf16[256,2048]{1,0:T(8,128)(2,1)} %pad_maximum_fusion.2), channel_id=1, source_target_pairs={{0,16},{1,17},{2,18},{3,19},{4,20},{5,21},{6,22},{7,23},{8,24},{9,... | collective-permute-start | bytes 3145736 | tf_op jit(solution)/shard_map/ppermute | solution.py:189
  179.2 57.6 %collective-permute-start.6 = (bf16[224,1024]{1,0:T(8,128)(2,1)}, bf16[224,1024]{1,0:T(8,128)(2,1)}, u32[]{:S(2)}, u32[]{:S(2)}) collective-permute-start(bf16[224,1024]{1,0:T(8,128)(2,1)} %copy_bitcast_fusion), channel_id=1, source_target_pairs={{0,256},{1,257},{2,258},{3,259},{4,260},{5,261},{6,262},{7,263},{8... | collective-permute-start | bytes 1376264 | tf_op jit(solution)/shard_map/ppermute | solution.py:213
  187.2 35.9 %collective-permute-start.5 = (bf16[256,2048]{1,0:T(8,128)(2,1)}, bf16[256,2048]{1,0:T(8,128)(2,1)S(1)}, u32[]{:S(2)}, u32[]{:S(2)}) collective-permute-start(bf16[256,2048]{1,0:T(8,128)(2,1)} %pad_maximum_fusion.2), channel_id=1, source_target_pairs={{0,24},{1,25},{2,26},{3,27},{4,28},{5,29},{6,30},{7,31},{8,0},{9,1... | collective-permute-start | bytes 3145736 | tf_op jit(solution)/shard_map/ppermute | solution.py:189
  224.1 1.2 copy-start.2
  232.2 28.3 %all-to-all-start.3 = ((bf16[4,4,128,256]{3,2,1,0:T(8,128)(2,1)}), bf16[4,4,128,256]{3,2,1,0:T(8,128)(2,1)S(1)}, u32[]{:S(2)}, u32[]{:S(2)}) async-start(bf16[4,4,128,256]{3,2,1,0:T(8,128)(2,1)} %get-tuple-element.15), calls=%async_computation.3 | async-start | bytes 2097152 | tf_op jit(solution)/shard_map/all_to_all | solution.py:246
  238.0 27.3 %copy-start = (bf16[4,128,224]{2,1,0:T(8,128)(2,1)S(1)}, bf16[4,128,224]{2,1,0:T(8,128)(2,1)}, u32[]{:S(2)}) copy-start(bf16[4,128,224]{2,1,0:T(8,128)(2,1)} %get-tuple-element.14.refs_0_) | copy-start | bytes 688132
  238.6 16.6 %collective-permute-start.10 = (bf16[224,512]{1,0:T(8,128)(2,1)S(1)}, bf16[224,512]{1,0:T(8,128)(2,1)S(1)}, u32[]{:S(2)}, u32[]{:S(2)}) collective-permute-start(bf16[224,512]{1,0:T(8,128)(2,1)S(1)} %get-tuple-element.34), channel_id=1, source_target_pairs={{0,8},{1,9},{2,10},{3,11},{4,12},{5,13},{6,14},{7,15},{8,16},{9,17... | collective-permute-start | bytes 688136 | tf_op jit(solution)/shard_map/ppermute | solution.py:189
  242.0 18.5 %collective-permute-start.11 = (bf16[224,512]{1,0:T(8,128)(2,1)S(1)}, bf16[224,512]{1,0:T(8,128)(2,1)S(1)}, u32[]{:S(2)}, u32[]{:S(2)}) collective-permute-start(bf16[224,512]{1,0:T(8,128)(2,1)S(1)} %get-tuple-element.35), channel_id=1, source_target_pairs={{0,16},{1,17},{2,18},{3,19},{4,20},{5,21},{6,22},{7,23},{8,24},{9,... | collective-permute-start | bytes 688136 | tf_op jit(solution)/shard_map/ppermute | solution.py:189
  246.3 14.2 %collective-permute-start.12 = (bf16[224,512]{1,0:T(8,128)(2,1)S(1)}, bf16[224,512]{1,0:T(8,128)(2,1)S(1)}, u32[]{:S(2)}, u32[]{:S(2)}) collective-permute-start(bf16[224,512]{1,0:T(8,128)(2,1)S(1)} %get-tuple-element.32), channel_id=1, source_target_pairs={{0,24},{1,25},{2,26},{3,27},{4,28},{5,29},{6,30},{7,31},{8,0},{9,1... | collective-permute-start | bytes 688136 | tf_op jit(solution)/shard_map/ppermute | solution.py:189
  261.2 22.9 %collective-permute-start.13 = (bf16[4,128,512]{2,1,0:T(8,128)(2,1)S(1)}, bf16[4,128,512]{2,1,0:T(8,128)(2,1)S(1)}, u32[]{:S(2)}, u32[]{:S(2)}) collective-permute-start(bf16[4,128,512]{2,1,0:T(8,128)(2,1)S(1)} %partial_out.3), channel_id=1, source_target_pairs={{0,480},{1,33},{2,482},{3,35},{4,484},{5,37},{6,486},{7,39},{8,488... | collective-permute-start | bytes 1572872 | tf_op jit(solution)/shard_map/ppermute | solution.py:186
  265.3 10.1 %collective-permute-start.7 = (bf16[4,128,224]{2,1,0:T(8,128)(2,1)S(1)}, bf16[4,128,224]{2,1,0:T(8,128)(2,1)S(1)}, u32[]{:S(2)}, u32[]{:S(2)}) collective-permute-start(bf16[4,128,224]{2,1,0:T(8,128)(2,1)S(1)} %copy-done), channel_id=1, source_target_pairs={{0,8},{1,9},{2,10},{3,11},{4,12},{5,13},{6,14},{7,15},{8,16},{9,17... | collective-permute-start | bytes 688136 | tf_op jit(solution)/shard_map/ppermute | solution.py:189
  269.2 13.1 %collective-permute-start.8 = (bf16[4,128,224]{2,1,0:T(8,128)(2,1)S(1)}, bf16[4,128,224]{2,1,0:T(8,128)(2,1)S(1)}, u32[]{:S(2)}, u32[]{:S(2)}) collective-permute-start(bf16[4,128,224]{2,1,0:T(8,128)(2,1)S(1)} %copy-done), channel_id=1, source_target_pairs={{0,16},{1,17},{2,18},{3,19},{4,20},{5,21},{6,22},{7,23},{8,24},{9,... | collective-permute-start | bytes 688136 | tf_op jit(solution)/shard_map/ppermute | solution.py:189
  272.9 10.4 %collective-permute-start.9 = (bf16[4,128,224]{2,1,0:T(8,128)(2,1)S(1)}, bf16[4,128,224]{2,1,0:T(8,128)(2,1)S(1)}, u32[]{:S(2)}, u32[]{:S(2)}) collective-permute-start(bf16[4,128,224]{2,1,0:T(8,128)(2,1)S(1)} %copy-done), channel_id=1, source_target_pairs={{0,24},{1,25},{2,26},{3,27},{4,28},{5,29},{6,30},{7,31},{8,0},{9,1... | collective-permute-start | bytes 688136 | tf_op jit(solution)/shard_map/ppermute | solution.py:189
  284.3 11.5 %collective-permute-start.14 = (bf16[4,64,512]{2,1,0:T(8,128)(2,1)S(1)}, bf16[4,64,512]{2,1,0:T(8,128)(2,1)S(1)}, u32[]{:S(2)}, u32[]{:S(2)}) collective-permute-start(bf16[4,64,512]{2,1,0:T(8,128)(2,1)S(1)} %slice.49), channel_id=1, source_target_pairs={{0,448},{1,65},{2,450},{3,67},{4,452},{5,69},{6,454},{7,71},{8,456... | collective-permute-start | bytes 786440 | tf_op jit(solution)/shard_map/ppermute | solution.py:186
  295.9 20.1 %copy-start.6 = (f32[128,2]{0,1:T(2,128)S(1)}, f32[128,2]{0,1:T(2,128)}, u32[]{:S(2)}) copy-start(f32[128,2]{0,1:T(2,128)} %param.9) | copy-start | bytes 3076
  296.0 12.8 %collective-permute-start.15 = (bf16[4,32,512]{2,1,0:T(8,128)(2,1)S(1)}, bf16[4,32,512]{2,1,0:T(8,128)(2,1)S(1)}, u32[]{:S(2)}, u32[]{:S(2)}) collective-permute-start(bf16[4,32,512]{2,1,0:T(8,128)(2,1)S(1)} %slice.50), channel_id=1, source_target_pairs={{0,384},{1,129},{2,386},{3,131},{4,388},{5,133},{6,390},{7,135},{8... | collective-permute-start | bytes 393224 | tf_op jit(solution)/shard_map/ppermute | solution.py:186
  309.9 23.2 %all-to-all-start.4 = ((bf16[32,32,512]{2,1,0:T(8,128)(2,1)}), bf16[32,32,512]{2,1,0:T(8,128)(2,1)S(1)}, u32[]{:S(2)}, u32[]{:S(2)}) async-start(bf16[32,32,512]{2,1,0:T(8,128)(2,1)} %bitcast.12), calls=%async_computation.4 | async-start | bytes 2097152 | tf_op jit(solution)/shard_map/all_to_all | solution.py:262
  316.1 3.5 %copy-start.3 = (bf16[1,2048,224]{2,1,0:T(8,128)(2,1)S(1)}, bf16[1,2048,224]{2,1,0:T(8,128)(2,1)}, u32[]{:S(2)}) copy-start(bf16[1,2048,224]{2,1,0:T(8,128)(2,1)} %get-tuple-element.29) | copy-start | bytes 2752516

commit v2 on v1

--- a/solution.py
+++ b/solution.py
@@ -164,6 +164,23 @@
     )(*first, *hidden, *down)
 
 
+def spread_kernel(total_ref, moved_ref, out_ref):
+    block = (total_ref[...] + moved_ref[...].astype(jnp.float32)).astype(jnp.bfloat16)
+    for t in range(out_ref.shape[1]):
+        out_ref[:, t] = block
+
+
+def spread(total, moved, copies):
+    pieces, rows, columns = total.shape
+    return pl.pallas_call(
+        spread_kernel,
+        out_shape=jax.ShapeDtypeStruct((pieces, copies, rows, columns), jnp.bfloat16),
+        cost_estimate=pl.CostEstimate(flops=65536, bytes_accessed=1500000, transcendentals=0),
+        compiler_params=pltpu.CompilerParams(vmem_limit_bytes=8 * 2**20),
+        name="spread",
+    )(total, moved)
+
+
 def permutation(sizes, move):
     groups, fs_0, fs_1, tp = sizes
     pairs = []
@@ -251,14 +268,13 @@
     total = partial_out(pieces, down_cols, f32)
     for hops in (1, 2, 4):
         moved = along_z(odd.astype(bf16), -hops)
-        total = total + moved.astype(f32)
-        half = total.shape[1] // 2
-        total, odd = total[:, :half], total[:, half:]
         if hops == 4:
-            total = jnp.concatenate([total, odd], axis=1)
-
-    block = total.astype(bf16)
-    block = jnp.broadcast_to(block[:, None], (fs_1, tp_size, *block.shape[1:]))
+            block = spread(total, moved, tp_size)
+        else:
+            total = total + moved.astype(f32)
+            half = total.shape[1] // 2
+            total, odd = total[:, :half], total[:, half:]
+
     blocks = lax.all_to_all(block.reshape(-1, *block.shape[2:]), ("fs_1", "tp"), 0, 0, tiled=True)
     blocks = blocks.reshape(fs_1, -1, columns).astype(f32) * slot_weight.reshape(1, -1, 1)
     blocks = jnp.moveaxis(blocks.astype(bf16), 0, 1).reshape(-1, fs_1 * columns)

time: 340 us -> 340 us (level)
  no operation moved by 1% of the time
where the time goes in v2:
time: 340 us; the launch traced here: 335 us
  waiting for transfers between devices  187 us (55%)
  starting transfers between devices  106 us (31%)
  local copies, waits for them, and re-layouts  15.7 us (5%)
  Pallas kernels  15.7 us (5%)
  other arithmetic  8.34 us (2%)
    ppermute x6, waiting for transfers between devices, along_z(): return lax.ppermute(x, ALL, pairs)  110 us
    ppermute x9, waiting for transfers between devices, along_y(): lax.ppermute(x, ALL, permutation(sizes, lambda z, y, t: (z, y + hops)))  44.8 us
    ppermute x9, starting transfers between devices, along_y(): lax.ppermute(x, ALL, permutation(sizes, lambda z, y, t: (z, y + hops)))  31.1 us
    ppermute x6, starting transfers between devices, along_z(): return lax.ppermute(x, ALL, pairs)  27.6 us
    all_to_all x1, starting transfers between devices, local(): tiles = lax.all_to_all(tiles, GR_FS, 0, 0, tiled=True)  13.9 us
    all_to_all x1, waiting for transfers between devices, local(): lax.all_to_all(tiles, 'tp', 0, 0, tiled=True).reshape(-1, 112, LANES)  12.8 us
    all_to_all x1, waiting for transfers between devices, local(): lax.all_to_all(block.reshape(-1, *block.shape[2:]), ('fs_1', 'tp'), 0, 0,...  12.3 us
    all_to_all x1, starting transfers between devices, local(): lax.all_to_all(tiles, 'tp', 0, 0, tiled=True).reshape(-1, 112, LANES)  10.3 us
  transfers between devices with their start and end apart: 21, of which 15 were waited for; matrix products, arithmetic and copies ran while one was open for 6% of the time, Pallas kernels for 2%

profile of v2, /device:TPU:1, one launch (start us, length us, event | category | flops | bytes accessed | tf_op | source)
XLA Modules:
  0.0 335.1 jit_solution(11928488846254317696)
XLA Ops:
  0.6 1.3 copy.30.gain_ref
  2.0 6.3 %pack.1 = bf16[8,448,128]{2,1,0:T(8,128)(2,1)} custom-call(f32[8,32,896]{2,1,0:T(8,128)} %gate_ref.1, f32[8,32,896]{2,1,0:T(8,128)} %up_ref.1, f32[32,1]{1,0:T(8,128)} %copy.30.gain_ref), custom_call_target="tpu_custom_call" | custom-call | flops 4000000 | bytes 2800000 | tf_op jit(solution)/shard_map/pack/pallas_call | solution.py:46
  8.3 10.3 %all-to-all-start = ((bf16[8,448,128]{2,1,0:T(8,128)(2,1)}), bf16[8,448,128]{2,1,0:T(8,128)(2,1)S(1)}, u32[]{:S(2)}, u32[]{:S(2)}) async-start(bf16[8,448,128]{2,1,0:T(8,128)(2,1)} %pack.1), calls=%async_computation | async-start | bytes 1835008 | tf_op jit(solution)/shard_map/all_to_all | solution.py:233
  19.4 12.8 %all-to-all-done = bf16[8,448,128]{2,1,0:T(8,128)(2,1)S(1)} async-done(((bf16[8,448,128]{2,1,0:T(8,128)(2,1)}), bf16[8,448,128]{2,1,0:T(8,128)(2,1)S(1)}, u32[]{:S(2)}, u32[]{:S(2)}) %all-to-all-start) | async-done | bytes 917536 | tf_op jit(solution)/shard_map/all_to_all | solution.py:233
  32.2 4.3 %all-to-all-start.2 = ((bf16[8,224,128]{2,1,0:T(8,128)(2,1)}), bf16[8,224,128]{2,1,0:T(8,128)(2,1)S(1)}, u32[]{:S(2)}, u32[]{:S(2)}) async-start(bf16[8,224,128]{2,1,0:T(8,128)(2,1)} %convert_element_type.45), calls=%async_computation.2 | async-start | bytes 917504 | tf_op jit(solution)/shard_map/all_to_all | solution.py:227
  36.5 1.4 pad_maximum_fusion
  37.9 7.3 %all-to-all-done.2 = bf16[8,224,128]{2,1,0:T(8,128)(2,1)S(1)} async-done(((bf16[8,224,128]{2,1,0:T(8,128)(2,1)}), bf16[8,224,128]{2,1,0:T(8,128)(2,1)S(1)}, u32[]{:S(2)}, u32[]{:S(2)}) %all-to-all-start.2) | async-done | bytes 458784 | tf_op jit(solution)/shard_map/all_to_all | solution.py:227
  45.2 13.9 %all-to-all-start.1 = ((bf16[64,112,128]{2,1,0:T(8,128)(2,1)}), bf16[64,112,128]{2,1,0:T(8,128)(2,1)S(1)}, u32[]{:S(2)}, u32[]{:S(2)}) async-start(bf16[64,112,128]{2,1,0:T(8,128)(2,1)} %pad_maximum_fusion), calls=%async_computation.1 | async-start | bytes 3670016 | tf_op jit(solution)/shard_map/all_to_all | solution.py:235
  60.0 7.0 %collective-permute-start = (bf16[32,2048]{1,0:T(8,128)(2,1)S(1)}, bf16[32,2048]{1,0:T(8,128)(2,1)S(1)}, u32[]{:S(2)}, u32[]{:S(2)}) collective-permute-start(bf16[32,2048]{1,0:T(8,128)(2,1)S(1)} %convolution_convert_fusion.1), channel_id=1, source_target_pairs={{0,128},{1,385},{2,130},{3,387},{4,132},{5,389},{6,134},{7,391},{8... | collective-permute-start | bytes 393224 | tf_op jit(solution)/shard_map/ppermute | solution.py:203
  67.0 81.2 %collective-permute-done = bf16[32,2048]{1,0:T(8,128)(2,1)S(1)} collective-permute-done((bf16[32,2048]{1,0:T(8,128)(2,1)S(1)}, bf16[32,2048]{1,0:T(8,128)(2,1)S(1)}, u32[]{:S(2)}, u32[]{:S(2)}) %collective-permute-start) | collective-permute-done | bytes 131104 | tf_op jit(solution)/shard_map/ppermute | solution.py:203
  148.2 1.9 collective-permute-start.1
  150.2 7.4 %collective-permute-done.1 = bf16[64,2048]{1,0:T(8,128)(2,1)S(1)} collective-permute-done((bf16[64,2048]{1,0:T(8,128)(2,1)S(1)}, bf16[64,2048]{1,0:T(8,128)(2,1)S(1)}, u32[]{:S(2)}, u32[]{:S(2)}) %collective-permute-start.1) | collective-permute-done | bytes 262176 | tf_op jit(solution)/shard_map/ppermute | solution.py:203
  157.6 4.2 %collective-permute-start.2 = (bf16[128,2048]{1,0:T(8,128)(2,1)S(1)}, bf16[128,2048]{1,0:T(8,128)(2,1)S(1)}, u32[]{:S(2)}, u32[]{:S(2)}) collective-permute-start(bf16[128,2048]{1,0:T(8,128)(2,1)S(1)} %pad_maximum_fusion.3), channel_id=1, source_target_pairs={{0,32},{1,481},{2,34},{3,483},{4,36},{5,485},{6,38},{7,487},{8,40}... | collective-permute-start | bytes 1572872 | tf_op jit(solution)/shard_map/ppermute | solution.py:203
  161.8 7.1 %collective-permute-done.2 = bf16[128,2048]{1,0:T(8,128)(2,1)S(1)} collective-permute-done((bf16[128,2048]{1,0:T(8,128)(2,1)S(1)}, bf16[128,2048]{1,0:T(8,128)(2,1)S(1)}, u32[]{:S(2)}, u32[]{:S(2)}) %collective-permute-start.2) | collective-permute-done | bytes 524320 | tf_op jit(solution)/shard_map/ppermute | solution.py:203
  169.9 3.0 collective-permute-start.3
  172.9 5.3 %collective-permute-start.4 = (bf16[256,2048]{1,0:T(8,128)(2,1)}, bf16[256,2048]{1,0:T(8,128)(2,1)}, u32[]{:S(2)}, u32[]{:S(2)}) collective-permute-start(bf16[256,2048]{1,0:T(8,128)(2,1)} %pad_maximum_fusion.2), channel_id=1, source_target_pairs={{0,16},{1,17},{2,18},{3,19},{4,20},{5,21},{6,22},{7,23},{8,24},{9,... | collective-permute-start | bytes 3145736 | tf_op jit(solution)/shard_map/ppermute | solution.py:206
  179.2 8.0 %collective-permute-start.6 = (bf16[224,1024]{1,0:T(8,128)(2,1)}, bf16[224,1024]{1,0:T(8,128)(2,1)}, u32[]{:S(2)}, u32[]{:S(2)}) collective-permute-start(bf16[224,1024]{1,0:T(8,128)(2,1)} %copy_bitcast_fusion), channel_id=1, source_target_pairs={{0,256},{1,257},{2,258},{3,259},{4,260},{5,261},{6,262},{7,263},{8... | collective-permute-start | bytes 1376264 | tf_op jit(solution)/shard_map/ppermute | solution.py:230
  187.2 1.9 collective-permute-start.5
  189.1 2.5 broadcast_in_dim.58
  192.6 1.6 collective-permute-done.3
  194.2 2.3 bitcast_dynamic-update-slice_fusion.2
  196.5 21.5 %collective-permute-done.4 = bf16[256,2048]{1,0:T(8,128)(2,1)} collective-permute-done((bf16[256,2048]{1,0:T(8,128)(2,1)}, bf16[256,2048]{1,0:T(8,128)(2,1)}, u32[]{:S(2)}, u32[]{:S(2)}) %collective-permute-start.4) | collective-permute-done | bytes 1048608 | tf_op jit(solution)/shard_map/ppermute | solution.py:206
  218.0 2.3 bitcast_dynamic-update-slice_fusion.1
  220.4 2.7 collective-permute-done.5
  224.1 1.2 copy-done.2
  225.3 6.9 %hidden_units.1 = (bf16[1,2048,224]{2,1,0:T(8,128)(2,1)}, bf16[1,2048,224]{2,1,0:T(8,128)(2,1)}, bf16[4,128,224]{2,1,0:T(8,128)(2,1)}, bf16[4,4,128,256]{3,2,1,0:T(8,128)(2,1)}) custom-call(bf16[64,112,128]{2,1,0:T(8,128)(2,1)} %copy-done.2, bf16[1024,2048]{1,0:T(8,128)(2,1)} %bitcast.7.tokens_ref), custom_call_target="tpu_custom_call" | custom-call | flops 1900000000 | bytes 8500000 | tf_op jit(solution)/shard_map/hidden_units/pallas_call | solution.py:99
  232.2 4.6 %all-to-all-start.3 = ((bf16[4,4,128,256]{3,2,1,0:T(8,128)(2,1)}), bf16[4,4,128,256]{3,2,1,0:T(8,128)(2,1)S(1)}, u32[]{:S(2)}, u32[]{:S(2)}) async-start(bf16[4,4,128,256]{3,2,1,0:T(8,128)(2,1)} %get-tuple-element.15), calls=%async_computation.3 | async-start | bytes 2097152 | tf_op jit(solution)/shard_map/all_to_all | solution.py:263
  236.8 1.2 broadcast_select_fusion.1
  238.6 3.4 %collective-permute-start.10 = (bf16[224,512]{1,0:T(8,128)(2,1)S(1)}, bf16[224,512]{1,0:T(8,128)(2,1)S(1)}, u32[]{:S(2)}, u32[]{:S(2)}) collective-permute-start(bf16[224,512]{1,0:T(8,128)(2,1)S(1)} %get-tuple-element.34), channel_id=1, source_target_pairs={{0,8},{1,9},{2,10},{3,11},{4,12},{5,13},{6,14},{7,15},{8,16},{9,17... | collective-permute-start | bytes 688136 | tf_op jit(solution)/shard_map/ppermute | solution.py:206
  242.0 4.3 %collective-permute-start.11 = (bf16[224,512]{1,0:T(8,128)(2,1)S(1)}, bf16[224,512]{1,0:T(8,128)(2,1)S(1)}, u32[]{:S(2)}, u32[]{:S(2)}) collective-permute-start(bf16[224,512]{1,0:T(8,128)(2,1)S(1)} %get-tuple-element.35), channel_id=1, source_target_pairs={{0,16},{1,17},{2,18},{3,19},{4,20},{5,21},{6,22},{7,23},{8,24},{9,... | collective-permute-start | bytes 688136 | tf_op jit(solution)/shard_map/ppermute | solution.py:206
  246.3 3.1 collective-permute-start.12
  249.4 5.8 %collective-permute-done.10.refs_5_.refs_1_ = bf16[224,512]{1,0:T(8,128)(2,1)S(1)} collective-permute-done((bf16[224,512]{1,0:T(8,128)(2,1)S(1)}, bf16[224,512]{1,0:T(8,128)(2,1)S(1)}, u32[]{:S(2)}, u32[]{:S(2)}) %collective-permute-start.10) | collective-permute-done | bytes 229408 | tf_op jit(solution)/shard_map/ppermute | solution.py:206
  255.2 5.3 %collective-permute-done.11.refs_6_.refs_2_ = bf16[224,512]{1,0:T(8,128)(2,1)S(1)} collective-permute-done((bf16[224,512]{1,0:T(8,128)(2,1)S(1)}, bf16[224,512]{1,0:T(8,128)(2,1)S(1)}, u32[]{:S(2)}, u32[]{:S(2)}) %collective-permute-start.11) | collective-permute-done | bytes 229408 | tf_op jit(solution)/shard_map/ppermute | solution.py:206
  261.2 4.1 %collective-permute-start.13 = (bf16[4,128,512]{2,1,0:T(8,128)(2,1)S(1)}, bf16[4,128,512]{2,1,0:T(8,128)(2,1)S(1)}, u32[]{:S(2)}, u32[]{:S(2)}) collective-permute-start(bf16[4,128,512]{2,1,0:T(8,128)(2,1)S(1)} %partial_out.3), channel_id=1, source_target_pairs={{0,480},{1,33},{2,482},{3,35},{4,484},{5,37},{6,486},{7,39},{8,488... | collective-permute-start | bytes 1572872 | tf_op jit(solution)/shard_map/ppermute | solution.py:203
  265.3 3.9 %collective-permute-start.7 = (bf16[4,128,224]{2,1,0:T(8,128)(2,1)S(1)}, bf16[4,128,224]{2,1,0:T(8,128)(2,1)S(1)}, u32[]{:S(2)}, u32[]{:S(2)}) collective-permute-start(bf16[4,128,224]{2,1,0:T(8,128)(2,1)S(1)} %copy-done), channel_id=1, source_target_pairs={{0,8},{1,9},{2,10},{3,11},{4,12},{5,13},{6,14},{7,15},{8,16},{9,17... | collective-permute-start | bytes 688136 | tf_op jit(solution)/shard_map/ppermute | solution.py:206
  269.2 3.7 %collective-permute-start.8 = (bf16[4,128,224]{2,1,0:T(8,128)(2,1)S(1)}, bf16[4,128,224]{2,1,0:T(8,128)(2,1)S(1)}, u32[]{:S(2)}, u32[]{:S(2)}) collective-permute-start(bf16[4,128,224]{2,1,0:T(8,128)(2,1)S(1)} %copy-done), channel_id=1, source_target_pairs={{0,16},{1,17},{2,18},{3,19},{4,20},{5,21},{6,22},{7,23},{8,24},{9,... | collective-permute-start | bytes 688136 | tf_op jit(solution)/shard_map/ppermute | solution.py:206
  272.9 2.5 collective-permute-start.9
  275.4 6.9 %collective-permute-done.8.refs_2_ = bf16[4,128,224]{2,1,0:T(8,128)(2,1)S(1)} collective-permute-done((bf16[4,128,224]{2,1,0:T(8,128)(2,1)S(1)}, bf16[4,128,224]{2,1,0:T(8,128)(2,1)S(1)}, u32[]{:S(2)}, u32[]{:S(2)}) %collective-permute-start.8) | collective-permute-done | bytes 229408 | tf_op jit(solution)/shard_map/ppermute | solution.py:206
  284.3 5.8 %collective-permute-start.14 = (bf16[4,64,512]{2,1,0:T(8,128)(2,1)S(1)}, bf16[4,64,512]{2,1,0:T(8,128)(2,1)S(1)}, u32[]{:S(2)}, u32[]{:S(2)}) collective-permute-start(bf16[4,64,512]{2,1,0:T(8,128)(2,1)S(1)} %slice.43), channel_id=1, source_target_pairs={{0,448},{1,65},{2,450},{3,67},{4,452},{5,69},{6,454},{7,71},{8,456... | collective-permute-start | bytes 786440 | tf_op jit(solution)/shard_map/ppermute | solution.py:203
  290.1 5.7 %collective-permute-done.14 = bf16[4,64,512]{2,1,0:T(8,128)(2,1)S(1)} collective-permute-done((bf16[4,64,512]{2,1,0:T(8,128)(2,1)S(1)}, bf16[4,64,512]{2,1,0:T(8,128)(2,1)S(1)}, u32[]{:S(2)}, u32[]{:S(2)}) %collective-permute-start.14) | collective-permute-done | bytes 262176 | tf_op jit(solution)/shard_map/ppermute | solution.py:203
  296.0 4.5 %collective-permute-start.15 = (bf16[4,32,512]{2,1,0:T(8,128)(2,1)S(1)}, bf16[4,32,512]{2,1,0:T(8,128)(2,1)S(1)}, u32[]{:S(2)}, u32[]{:S(2)}) collective-permute-start(bf16[4,32,512]{2,1,0:T(8,128)(2,1)S(1)} %slice.44), channel_id=1, source_target_pairs={{0,384},{1,129},{2,386},{3,131},{4,388},{5,133},{6,390},{7,135},{8... | collective-permute-start | bytes 393224 | tf_op jit(solution)/shard_map/ppermute | solution.py:203
  300.5 8.2 %collective-permute-done.15.moved_ref = bf16[4,32,512]{2,1,0:T(8,128)(2,1)S(1)} collective-permute-done((bf16[4,32,512]{2,1,0:T(8,128)(2,1)S(1)}, bf16[4,32,512]{2,1,0:T(8,128)(2,1)S(1)}, u32[]{:S(2)}, u32[]{:S(2)}) %collective-permute-start.15) | collective-permute-done | bytes 131104 | tf_op jit(solution)/shard_map/ppermute | solution.py:203
  308.8 1.1 spread.1
  309.8 6.1 %all-to-all-start.4 = ((bf16[32,32,512]{2,1,0:T(8,128)(2,1)}), bf16[32,32,512]{2,1,0:T(8,128)(2,1)S(1)}, u32[]{:S(2)}, u32[]{:S(2)}) async-start(bf16[32,32,512]{2,1,0:T(8,128)(2,1)} %bitcast.12), calls=%async_computation.4 | async-start | bytes 2097152 | tf_op jit(solution)/shard_map/all_to_all | solution.py:278
  317.3 2.2 copy.33
  319.5 1.3 copy.34
  320.7 12.3 %all-to-all-done.4 = bf16[32,32,512]{2,1,0:T(8,128)(2,1)S(1)} async-done(((bf16[32,32,512]{2,1,0:T(8,128)(2,1)}), bf16[32,32,512]{2,1,0:T(8,128)(2,1)S(1)}, u32[]{:S(2)}, u32[]{:S(2)}) %all-to-all-start.4) | async-done | bytes 1048608 | tf_op jit(solution)/shard_map/all_to_all | solution.py:278
  333.8 1.3 convolution_convert_fusion
  (52 shorter events, 11.0 us)
Async XLA Ops:
  2.0 16.6 %copy-start.4 = (f32[8,224,128]{2,1,0:T(8,128)S(1)}, f32[8,224,128]{2,1,0:T(8,128)}, u32[]{:S(2)}) copy-start(f32[8,224,128]{2,1,0:T(8,128)} %param.13) | copy-start | bytes 2752516
  8.3 23.9 %all-to-all-start = ((bf16[8,448,128]{2,1,0:T(8,128)(2,1)}), bf16[8,448,128]{2,1,0:T(8,128)(2,1)S(1)}, u32[]{:S(2)}, u32[]{:S(2)}) async-start(bf16[8,448,128]{2,1,0:T(8,128)(2,1)} %pack.1), calls=%async_computation | async-start | bytes 1835008 | tf_op jit(solution)/shard_map/all_to_all | solution.py:233
  32.2 13.0 %all-to-all-start.2 = ((bf16[8,224,128]{2,1,0:T(8,128)(2,1)}), bf16[8,224,128]{2,1,0:T(8,128)(2,1)S(1)}, u32[]{:S(2)}, u32[]{:S(2)}) async-start(bf16[8,224,128]{2,1,0:T(8,128)(2,1)} %convert_element_type.45), calls=%async_computation.2 | async-start | bytes 917504 | tf_op jit(solution)/shard_map/all_to_all | solution.py:227
  37.9 21.2 %copy-start.5 = (s32[128,2]{0,1:T(2,128)S(1)}, s32[128,2]{0,1:T(2,128)}, u32[]{:S(2)}) copy-start(s32[128,2]{0,1:T(2,128)} %param.8) | copy-start | bytes 3076
  37.9 21.5 %copy-start.1 = (bf16[128,2048]{1,0:T(8,128)(2,1)S(1)}, bf16[128,2048]{1,0:T(8,128)(2,1)}, u32[]{:S(2)}) copy-start(bf16[128,2048]{1,0:T(8,128)(2,1)} %param.7) | copy-start | bytes 1572868
  45.2 178.9 %all-to-all-start.1 = ((bf16[64,112,128]{2,1,0:T(8,128)(2,1)}), bf16[64,112,128]{2,1,0:T(8,128)(2,1)S(1)}, u32[]{:S(2)}, u32[]{:S(2)}) async-start(bf16[64,112,128]{2,1,0:T(8,128)(2,1)} %pad_maximum_fusion), calls=%async_computation.1 | async-start | bytes 3670016 | tf_op jit(solution)/shard_map/all_to_all | solution.py:235
  60.0 88.2 %collective-permute-start = (bf16[32,2048]{1,0:T(8,128)(2,1)S(1)}, bf16[32,2048]{1,0:T(8,128)(2,1)S(1)}, u32[]{:S(2)}, u32[]{:S(2)}) collective-permute-start(bf16[32,2048]{1,0:T(8,128)(2,1)S(1)} %convolution_convert_fusion.1), channel_id=1, source_target_pairs={{0,128},{1,385},{2,130},{3,387},{4,132},{5,389},{6,134},{7,391},{8... | collective-permute-start | bytes 393224 | tf_op jit(solution)/shard_map/ppermute | solution.py:203
  148.2 9.3 %collective-permute-start.1 = (bf16[64,2048]{1,0:T(8,128)(2,1)S(1)}, bf16[64,2048]{1,0:T(8,128)(2,1)S(1)}, u32[]{:S(2)}, u32[]{:S(2)}) collective-permute-start(bf16[64,2048]{1,0:T(8,128)(2,1)S(1)} %pad_maximum_fusion.4), channel_id=1, source_target_pairs={{0,64},{1,449},{2,66},{3,451},{4,68},{5,453},{6,70},{7,455},{8,72}... | collective-permute-start | bytes 786440 | tf_op jit(solution)/shard_map/ppermute | solution.py:203
  157.6 11.3 %collective-permute-start.2 = (bf16[128,2048]{1,0:T(8,128)(2,1)S(1)}, bf16[128,2048]{1,0:T(8,128)(2,1)S(1)}, u32[]{:S(2)}, u32[]{:S(2)}) collective-permute-start(bf16[128,2048]{1,0:T(8,128)(2,1)S(1)} %pad_maximum_fusion.3), channel_id=1, source_target_pairs={{0,32},{1,481},{2,34},{3,483},{4,36},{5,485},{6,38},{7,487},{8,40}... | collective-permute-start | bytes 1572872 | tf_op jit(solution)/shard_map/ppermute | solution.py:203
  169.9 24.3 %collective-permute-start.3 = (bf16[256,2048]{1,0:T(8,128)(2,1)}, bf16[256,2048]{1,0:T(8,128)(2,1)}, u32[]{:S(2)}, u32[]{:S(2)}) collective-permute-start(bf16[256,2048]{1,0:T(8,128)(2,1)} %pad_maximum_fusion.2), channel_id=1, source_target_pairs={{0,8},{1,9},{2,10},{3,11},{4,12},{5,13},{6,14},{7,15},{8,16},{9,17... | collective-permute-start | bytes 3145736 | tf_op jit(solution)/shard_map/ppermute | solution.py:206
  172.9 45.1 %collective-permute-start.4 = (bf16[256,2048]{1,0:T(8,128)(2,1)}, bf16[256,2048]{1,0:T(8,128)(2,1)}, u32[]{:S(2)}, u32[]{:S(2)}) collective-permute-start(bf16[256,2048]{1,0:T(8,128)(2,1)} %pad_maximum_fusion.2), channel_id=1, source_target_pairs={{0,16},{1,17},{2,18},{3,19},{4,20},{5,21},{6,22},{7,23},{8,24},{9,... | collective-permute-start | bytes 3145736 | tf_op jit(solution)/shard_map/ppermute | solution.py:206
  179.2 57.6 %collective-permute-start.6 = (bf16[224,1024]{1,0:T(8,128)(2,1)}, bf16[224,1024]{1,0:T(8,128)(2,1)}, u32[]{:S(2)}, u32[]{:S(2)}) collective-permute-start(bf16[224,1024]{1,0:T(8,128)(2,1)} %copy_bitcast_fusion), channel_id=1, source_target_pairs={{0,256},{1,257},{2,258},{3,259},{4,260},{5,261},{6,262},{7,263},{8... | collective-permute-start | bytes 1376264 | tf_op jit(solution)/shard_map/ppermute | solution.py:230
  187.2 35.9 %collective-permute-start.5 = (bf16[256,2048]{1,0:T(8,128)(2,1)}, bf16[256,2048]{1,0:T(8,128)(2,1)S(1)}, u32[]{:S(2)}, u32[]{:S(2)}) collective-permute-start(bf16[256,2048]{1,0:T(8,128)(2,1)} %pad_maximum_fusion.2), channel_id=1, source_target_pairs={{0,24},{1,25},{2,26},{3,27},{4,28},{5,29},{6,30},{7,31},{8,0},{9,1... | collective-permute-start | bytes 3145736 | tf_op jit(solution)/shard_map/ppermute | solution.py:206
  224.1 1.2 copy-start.2
  232.2 28.3 %all-to-all-start.3 = ((bf16[4,4,128,256]{3,2,1,0:T(8,128)(2,1)}), bf16[4,4,128,256]{3,2,1,0:T(8,128)(2,1)S(1)}, u32[]{:S(2)}, u32[]{:S(2)}) async-start(bf16[4,4,128,256]{3,2,1,0:T(8,128)(2,1)} %get-tuple-element.15), calls=%async_computation.3 | async-start | bytes 2097152 | tf_op jit(solution)/shard_map/all_to_all | solution.py:263
  238.0 27.3 %copy-start = (bf16[4,128,224]{2,1,0:T(8,128)(2,1)S(1)}, bf16[4,128,224]{2,1,0:T(8,128)(2,1)}, u32[]{:S(2)}) copy-start(bf16[4,128,224]{2,1,0:T(8,128)(2,1)} %get-tuple-element.14.refs_0_) | copy-start | bytes 688132
  238.6 16.6 %collective-permute-start.10 = (bf16[224,512]{1,0:T(8,128)(2,1)S(1)}, bf16[224,512]{1,0:T(8,128)(2,1)S(1)}, u32[]{:S(2)}, u32[]{:S(2)}) collective-permute-start(bf16[224,512]{1,0:T(8,128)(2,1)S(1)} %get-tuple-element.34), channel_id=1, source_target_pairs={{0,8},{1,9},{2,10},{3,11},{4,12},{5,13},{6,14},{7,15},{8,16},{9,17... | collective-permute-start | bytes 688136 | tf_op jit(solution)/shard_map/ppermute | solution.py:206
  242.0 18.5 %collective-permute-start.11 = (bf16[224,512]{1,0:T(8,128)(2,1)S(1)}, bf16[224,512]{1,0:T(8,128)(2,1)S(1)}, u32[]{:S(2)}, u32[]{:S(2)}) collective-permute-start(bf16[224,512]{1,0:T(8,128)(2,1)S(1)} %get-tuple-element.35), channel_id=1, source_target_pairs={{0,16},{1,17},{2,18},{3,19},{4,20},{5,21},{6,22},{7,23},{8,24},{9,... | collective-permute-start | bytes 688136 | tf_op jit(solution)/shard_map/ppermute | solution.py:206
  246.3 14.2 %collective-permute-start.12 = (bf16[224,512]{1,0:T(8,128)(2,1)S(1)}, bf16[224,512]{1,0:T(8,128)(2,1)S(1)}, u32[]{:S(2)}, u32[]{:S(2)}) collective-permute-start(bf16[224,512]{1,0:T(8,128)(2,1)S(1)} %get-tuple-element.32), channel_id=1, source_target_pairs={{0,24},{1,25},{2,26},{3,27},{4,28},{5,29},{6,30},{7,31},{8,0},{9,1... | collective-permute-start | bytes 688136 | tf_op jit(solution)/shard_map/ppermute | solution.py:206
  261.2 22.9 %collective-permute-start.13 = (bf16[4,128,512]{2,1,0:T(8,128)(2,1)S(1)}, bf16[4,128,512]{2,1,0:T(8,128)(2,1)S(1)}, u32[]{:S(2)}, u32[]{:S(2)}) collective-permute-start(bf16[4,128,512]{2,1,0:T(8,128)(2,1)S(1)} %partial_out.3), channel_id=1, source_target_pairs={{0,480},{1,33},{2,482},{3,35},{4,484},{5,37},{6,486},{7,39},{8,488... | collective-permute-start | bytes 1572872 | tf_op jit(solution)/shard_map/ppermute | solution.py:203
  265.3 10.1 %collective-permute-start.7 = (bf16[4,128,224]{2,1,0:T(8,128)(2,1)S(1)}, bf16[4,128,224]{2,1,0:T(8,128)(2,1)S(1)}, u32[]{:S(2)}, u32[]{:S(2)}) collective-permute-start(bf16[4,128,224]{2,1,0:T(8,128)(2,1)S(1)} %copy-done), channel_id=1, source_target_pairs={{0,8},{1,9},{2,10},{3,11},{4,12},{5,13},{6,14},{7,15},{8,16},{9,17... | collective-permute-start | bytes 688136 | tf_op jit(solution)/shard_map/ppermute | solution.py:206
  269.2 13.1 %collective-permute-start.8 = (bf16[4,128,224]{2,1,0:T(8,128)(2,1)S(1)}, bf16[4,128,224]{2,1,0:T(8,128)(2,1)S(1)}, u32[]{:S(2)}, u32[]{:S(2)}) collective-permute-start(bf16[4,128,224]{2,1,0:T(8,128)(2,1)S(1)} %copy-done), channel_id=1, source_target_pairs={{0,16},{1,17},{2,18},{3,19},{4,20},{5,21},{6,22},{7,23},{8,24},{9,... | collective-permute-start | bytes 688136 | tf_op jit(solution)/shard_map/ppermute | solution.py:206
  272.9 10.4 %collective-permute-start.9 = (bf16[4,128,224]{2,1,0:T(8,128)(2,1)S(1)}, bf16[4,128,224]{2,1,0:T(8,128)(2,1)S(1)}, u32[]{:S(2)}, u32[]{:S(2)}) collective-permute-start(bf16[4,128,224]{2,1,0:T(8,128)(2,1)S(1)} %copy-done), channel_id=1, source_target_pairs={{0,24},{1,25},{2,26},{3,27},{4,28},{5,29},{6,30},{7,31},{8,0},{9,1... | collective-permute-start | bytes 688136 | tf_op jit(solution)/shard_map/ppermute | solution.py:206
  284.3 11.5 %collective-permute-start.14 = (bf16[4,64,512]{2,1,0:T(8,128)(2,1)S(1)}, bf16[4,64,512]{2,1,0:T(8,128)(2,1)S(1)}, u32[]{:S(2)}, u32[]{:S(2)}) collective-permute-start(bf16[4,64,512]{2,1,0:T(8,128)(2,1)S(1)} %slice.43), channel_id=1, source_target_pairs={{0,448},{1,65},{2,450},{3,67},{4,452},{5,69},{6,454},{7,71},{8,456... | collective-permute-start | bytes 786440 | tf_op jit(solution)/shard_map/ppermute | solution.py:203
  295.9 20.0 %copy-start.6 = (f32[128,2]{0,1:T(2,128)S(1)}, f32[128,2]{0,1:T(2,128)}, u32[]{:S(2)}) copy-start(f32[128,2]{0,1:T(2,128)} %param.9) | copy-start | bytes 3076
  296.0 12.8 %collective-permute-start.15 = (bf16[4,32,512]{2,1,0:T(8,128)(2,1)S(1)}, bf16[4,32,512]{2,1,0:T(8,128)(2,1)S(1)}, u32[]{:S(2)}, u32[]{:S(2)}) collective-permute-start(bf16[4,32,512]{2,1,0:T(8,128)(2,1)S(1)} %slice.44), channel_id=1, source_target_pairs={{0,384},{1,129},{2,386},{3,131},{4,388},{5,133},{6,390},{7,135},{8... | collective-permute-start | bytes 393224 | tf_op jit(solution)/shard_map/ppermute | solution.py:203
  309.8 23.2 %all-to-all-start.4 = ((bf16[32,32,512]{2,1,0:T(8,128)(2,1)}), bf16[32,32,512]{2,1,0:T(8,128)(2,1)S(1)}, u32[]{:S(2)}, u32[]{:S(2)}) async-start(bf16[32,32,512]{2,1,0:T(8,128)(2,1)} %bitcast.12), calls=%async_computation.4 | async-start | bytes 2097152 | tf_op jit(solution)/shard_map/all_to_all | solution.py:278
  316.0 3.5 %copy-start.3 = (bf16[1,2048,224]{2,1,0:T(8,128)(2,1)S(1)}, bf16[1,2048,224]{2,1,0:T(8,128)(2,1)}, u32[]{:S(2)}) copy-start(bf16[1,2048,224]{2,1,0:T(8,128)(2,1)} %get-tuple-element.29) | copy-start | bytes 2752516
